TPU v7x, 32 devices: a whole 2x2x4 slice. The times are simulated.
32 devices in a mesh: ep: 8 (over z, core), tp: 4 (over y, x).
Axes of the slice: x: 2, y: 2, z: 4, core: 2. Of those that a mesh axis runs over, the one named last changes fastest.
Arguments:
- query_pairs: bfloat16 [3072, 2048], P('ep', 'tp'), may hold values from -64 to 64
- key_pairs: bfloat16 [3072, 2048], P('ep', 'tp'), may hold values from -64 to 64
- value_rows: bfloat16 [3072, 2048], P('ep', 'tp'), may hold values from -6 to 6
- head_lambda: float32 [16], P('tp'), may hold values from 0.3 to 0.8
- head_gain: float32 [128], replicated, may hold values from 0.1 to 1.9
- out_weight: bfloat16 [2048, 2048], P('tp'), may hold values from -0.1875 to 0.1875
- moe_input: bfloat16 [1280, 2048], P('ep'), may hold values from -6 to 6
- ffn_gain: float32 [2048], replicated, may hold values from 0.1 to 1.9
- routes: int32 [1280, 2], P('ep'), may hold values from 0 to 7, all different within a row; in each aligned block of 160 rows (0 to 159, 160 to 319, ...) at most 50 rows name the same one
- route_weight: float32 [1280, 2], P('ep'), may hold values from 0.25 to 2.5
- gate_weight: bfloat16 [8, 2048, 2048], P('ep', None, 'tp'), may hold values from -0.125 to 0.125
- up_weight: bfloat16 [8, 2048, 2048], P('ep', None, 'tp'), may hold values from -0.125 to 0.125
- down_weight: bfloat16 [8, 2048, 2048], P('ep', 'tp'), may hold values from -0.1875 to 0.1875
- shared_gate: bfloat16 [2048, 2048], P(None, 'tp'), may hold values from -0.125 to 0.125
- shared_up: bfloat16 [2048, 2048], P(None, 'tp'), may hold values from -0.125 to 0.125
- shared_down: bfloat16 [2048, 2048], P('tp'), may hold values from -0.1875 to 0.1875
Outputs:
- attn_out: bfloat16 [3072, 2048], P('ep', 'tp')
- moe_out: bfloat16 [1280, 2048], P('ep', 'tp')
Inputs may be any that keep to these rules, and one draw needn't show every extreme that they name: `routes`: in each aligned block of 160 rows (the rows of one device along ep) no expert is named more than 50 times, a bound that some block reaches; a row names 2 different experts.
All inputs are finite; a program needn't handle non-finite values.
Results may differ from a plain program's by a relative error of at most 0.017.
The roundings to bfloat16 on the way count: a program that leaves them out, or rounds other values in their place, can miss the bound.
Values may be sent and summed in bfloat16 or wider, within the bound.
A program may use at most 64 MiB of HBM per device.

v0:
```python
import functools

import jax
import jax.numpy as jnp
from jax import lax
from jax.experimental import pallas as pl
from jax.experimental.pallas import tpu as pltpu
from jax.sharding import PartitionSpec as P

TOP_K = 2
KEY_BLOCK = 128


theta_base = 500000.0
norm_eps = 1e-06
masked_low = -1e30


def rotate(inputs, positions):
    half_size = inputs.shape[-1] // 2
    frequency = theta_base ** (-(jnp.arange(half_size, dtype=jnp.float32) * 2.0) / inputs.shape[-1])
    angles = positions.astype(jnp.float32)[:, None] * frequency[None, :]
    cosine = jnp.cos(angles)[:, None, None, :]
    sine_part = jnp.sin(angles)[:, None, None, :]
    front_half = inputs[..., :half_size]
    back_half = inputs[..., half_size:]
    return jnp.concatenate(
        [front_half * cosine - back_half * sine_part, back_half * cosine + front_half * sine_part],
        axis=-1,
    )


def generic_attention(query_pairs, key_pairs, value_rows, head_lambda, head_gain, out_weight):
    local_rows = query_pairs.shape[0]
    local_heads = head_lambda.shape[0]
    head_size = query_pairs.shape[1] // (2 * local_heads)
    value_size = value_rows.shape[1] // local_heads
    positions = lax.axis_index("ep") * local_rows + jnp.arange(local_rows, dtype=jnp.int32)
    rot_queries = rotate(
        query_pairs.astype(jnp.float32).reshape(local_rows, local_heads, 2, head_size), positions
    ).astype(jnp.bfloat16)
    rot_keys = rotate(
        key_pairs.astype(jnp.float32).reshape(local_rows, local_heads, 2, head_size), positions
    ).astype(jnp.bfloat16)
    rot_keys = rot_keys.reshape(local_rows, local_heads * 2 * head_size)
    zero_init = (
        jnp.full((local_heads, 2, local_rows), masked_low, jnp.float32),
        jnp.zeros((local_heads, 2, local_rows), jnp.float32),
        jnp.zeros((local_heads, 2, local_rows, value_size), jnp.float32),
    )
    piece_keys = lax.all_gather(rot_keys, "ep", axis=0, tiled=True)
    piece_values = lax.all_gather(value_rows, "ep", axis=0, tiled=True)
    block_count = piece_keys.shape[0] // KEY_BLOCK
    group_size = 4
    group_count = block_count // group_size
    grouped_keys = piece_keys.reshape(group_count, group_size, KEY_BLOCK, local_heads, 2, head_size)
    grouped_values = piece_values.reshape(
        group_count, group_size, KEY_BLOCK, local_heads, value_size
    )

    def one_group(current, inputs):
        block_keys, block_values, group_index = inputs
        key_positions = group_index * group_size * KEY_BLOCK + jnp.arange(
            group_size * KEY_BLOCK, dtype=jnp.int32
        ).reshape(group_size, KEY_BLOCK)
        scores = jnp.einsum(
            "qhmd,gkhmd->hmqgk", rot_queries, block_keys, preferred_element_type=jnp.float32
        ) * head_size ** (-0.5)
        allowed = key_positions[None, :, :] <= positions[:, None, None]
        scores = jnp.where(allowed, scores, masked_low)
        block_max = jnp.max(scores, axis=-1)
        weights = jnp.where(allowed, jnp.exp(scores - block_max[..., None]), 0.0)
        block_sum = jnp.sum(weights, axis=-1)
        block_out = jnp.einsum(
            "hmqgk,gkhc->hmqgc",
            weights.astype(jnp.bfloat16),
            block_values,
            preferred_element_type=jnp.float32,
        )
        run_max, run_sum, run_out = current
        new_max = jnp.maximum(run_max, jnp.max(block_max, axis=-1))
        old_scale = jnp.exp(run_max - new_max)
        new_scale = jnp.exp(block_max - new_max[..., None])
        run_sum = run_sum * old_scale + jnp.sum(new_scale * block_sum, axis=-1)
        run_out = run_out * old_scale[..., None] + jnp.sum(
            new_scale[..., None] * block_out, axis=-2
        )
        return ((new_max, run_sum, run_out), None)

    result, _ = lax.scan(
        one_group,
        zero_init,
        (grouped_keys, grouped_values, jnp.arange(group_count, dtype=jnp.int32)),
    )
    run_max, run_sum, run_out = result
    map_outputs = run_out / run_sum[..., None]
    difference = map_outputs[:, 0] - head_lambda[:, None, None] * map_outputs[:, 1]
    inverse_rms = lax.rsqrt(jnp.mean(difference * difference, axis=-1, keepdims=True) + norm_eps)
    normed_heads = (difference * inverse_rms * head_gain).astype(jnp.bfloat16)
    head_rows = normed_heads.transpose(1, 0, 2).reshape(local_rows, local_heads * value_size)
    mixer_terms = jnp.dot(head_rows, out_weight, preferred_element_type=jnp.float32)
    attn_out = lax.psum_scatter(
        mixer_terms.astype(jnp.bfloat16), "tp", scatter_dimension=1, tiled=True
    )
    return attn_out


MESH = pl.DeviceIdType.MESH
f32, bf16 = jnp.float32, jnp.bfloat16


def rotate_kernel(head_size, scale, q_ref, k_ref, cos_ref, sin_ref, rq_ref, rk_ref):
    heads, _, width = rq_ref.shape
    half = head_size // 2
    lane = lax.broadcasted_iota(jnp.int32, (q_ref.shape[0], width), 1)
    front = lane % head_size < half
    cosine, sine = cos_ref[...], sin_ref[...]
    for source, target, factor in ((q_ref, rq_ref, scale), (k_ref, rk_ref, 1.0)):
        for h in range(heads):
            x = source[:, h * width : (h + 1) * width].astype(f32)
            partner = jnp.where(front, pltpu.roll(x, width - half, 1), pltpu.roll(x, half, 1))
            turned = (x * cosine + partner * sine).astype(bf16)
            target[h] = turned if factor == 1.0 else turned * jnp.asarray(factor, bf16)


def attention_kernel(
    n, heads, lam_ref, gain_ref, rq_ref, rk_ref, v_ref, w_ref, tok_ref, out_ref, arr_ref,
    q_buf, k_buf, v_buf, vt_buf, hn_send, hn_buf, w_buf, acc, m_buf, l_buf,
    q_ss, q_rs, k_ss, k_rs, v_ss, v_rs, fk_ss, fk_rs, fv_ss, fv_rs, h_ss, h_rs, loc, w_sem, t_ss, t_rs, x_ss, x_rs,
):
    me = lax.axis_index("ep")
    my_tp = lax.axis_index("tp")
    n_tp = arr_ref.shape[0]
    g = n // heads
    my_head, my_core = me // g, me % g
    rows = rk_ref.shape[1]
    sub = rows // g
    width = rk_ref.shape[2]
    vw = v_buf.shape[2]

    barrier = pltpu.get_barrier_semaphore()
    for step in range(1, n):
        pl.semaphore_signal(barrier, inc=1, device_id={"ep": lax.rem(me + step, n)}, device_id_type=MESH)
    for step in range(1, n_tp):
        pl.semaphore_signal(barrier, inc=1, device_id={"tp": lax.rem(my_tp + step, n_tp)}, device_id_type=MESH)
    w_copy = pltpu.make_async_copy(w_ref, w_buf, w_sem)
    w_copy.start()

    def q_src(dest):
        start = pl.multiple_of(((dest % g + me) % g) * sub, sub)
        return rq_ref.at[dest // g, pl.ds(start, sub), :]

    def v_src(dest):
        return v_ref.at[:, pl.ds(pl.multiple_of((dest // g) * vw, vw), vw)]

    own = (
        pltpu.make_async_copy(q_src(me), q_buf.at[me], loc.at[0]),
        pltpu.make_async_copy(rk_ref.at[my_head], k_buf.at[me], loc.at[1]),
        pltpu.make_async_copy(v_src(me), v_buf.at[me], loc.at[2]),
        pltpu.make_async_copy(tok_ref.at[me], arr_ref.at[my_tp, me], loc.at[3]),
    )
    for copy in own:
        copy.start()
    pl.semaphore_wait(barrier, n - 1 + n_tp - 1)

    def q_copy(dest):
        return pltpu.make_async_remote_copy(
            q_src(dest), q_buf.at[me], q_ss.at[dest], q_rs.at[me],
            device_id={"ep": dest}, device_id_type=MESH)

    def k_copy(dest):
        return pltpu.make_async_remote_copy(
            rk_ref.at[dest // g], k_buf.at[me], k_ss.at[dest], k_rs.at[me],
            device_id={"ep": dest}, device_id_type=MESH)

    def v_copy(dest):
        return pltpu.make_async_remote_copy(
            v_src(dest), v_buf.at[me], v_ss.at[dest], v_rs.at[me],
            device_id={"ep": dest}, device_id_type=MESH)

    def tok_copy(dest):
        return pltpu.make_async_remote_copy(
            tok_ref.at[dest], arr_ref.at[my_tp, me], t_ss.at[dest], t_rs.at[me],
            device_id={"ep": dest}, device_id_type=MESH)

    def tok_arrival(source):
        return pltpu.make_async_remote_copy(
            tok_ref.at[0], arr_ref.at[my_tp, source], t_ss.at[0], t_rs.at[source],
            device_id={"ep": lax.rem(me + 1, n)}, device_id_type=MESH)

    def tok_spread(dest):
        return pltpu.make_async_remote_copy(
            arr_ref.at[my_tp], arr_ref.at[my_tp], x_ss.at[dest], x_rs.at[my_tp],
            device_id={"tp": dest}, device_id_type=MESH)

    def spread_arrival(source):
        return pltpu.make_async_remote_copy(
            arr_ref.at[source], arr_ref.at[source], x_ss.at[source], x_rs.at[source],
            device_id={"tp": lax.rem(my_tp + 1, n_tp)}, device_id_type=MESH)

    for step in range(1, n):
        tok_copy(lax.rem(me + step, n)).start()
    for step in range(1, n):
        dest = lax.rem(me + step, n)
        if step % g == 0:
            k_copy(dest).start()
            v_copy(dest).start()
        q_copy(dest).start()

    def mate(step):
        return my_head * g + lax.rem(my_core + step, g)

    def recv(buf, sem, source):
        return pltpu.make_async_remote_copy(
            buf.at[source], buf.at[source], sem.at[source], sem.at[source],
            device_id={"ep": lax.rem(me + 1, n)}, device_id_type=MESH)

    def forward(source, step):
        to = mate(step)
        return (
            pltpu.make_async_remote_copy(
                k_buf.at[source], k_buf.at[source], fk_ss.at[source, step], fk_rs.at[source],
                device_id={"ep": to}, device_id_type=MESH),
            pltpu.make_async_remote_copy(
                v_buf.at[source], v_buf.at[source], fv_ss.at[source, step], fv_rs.at[source],
                device_id={"ep": to}, device_id_type=MESH),
        )

    for copy in own:
        copy.wait()

    lam = lam_ref[my_head]
    gain = gain_ref[...]
    key_row = lax.broadcasted_iota(jnp.int32, (rows, g_cols(sub)), 0)
    query_col = lax.broadcasted_iota(jnp.int32, (rows, g_cols(sub)), 1) % sub
    lane = lax.broadcasted_iota(jnp.int32, (sub, width), 1)

    def group(p, _):
        direct = p * g + my_core

        @pl.when(direct != me)
        def _():
            recv(k_buf, k_rs, direct).wait_recv()
            recv(v_buf, v_rs, direct).wait_recv()

        for step in range(1, g):
            for copy in forward(direct, step):
                copy.start()
        for step in range(1, g):
            other = p * g + lax.rem(my_core + step, g)
            recv(k_buf, fk_rs, other).wait_recv()
            recv(v_buf, fv_rs, other).wait_recv()

        def member(c, _):
            e = p * g + c
            vt_buf[e] = v_buf[e].astype(f32).T.astype(bf16)

            @pl.when(e != me)
            def _():
                recv(q_buf, q_rs, e).wait_recv()

            q = q_buf[e]
            zero = jnp.zeros_like(q)
            stacked = jnp.concatenate(
                [jnp.where(lane < width // 2, q, zero), jnp.where(lane < width // 2, zero, q)], axis=0)
            q_start = ((my_core + e) % g) * sub

            def scores_of(j):
                return lax.dot_general(
                    k_buf[j], stacked, (((1,), (1,)), ((), ())), preferred_element_type=f32)

            s = jnp.where(key_row <= query_col + q_start, scores_of(e), masked_low)
            m = jnp.max(s, axis=0, keepdims=True)
            weights = jnp.exp(s - m)
            l_buf[...] = jnp.sum(weights, axis=0, keepdims=True)
            m_buf[...] = m
            acc[...] = jnp.dot(vt_buf[e], weights.astype(bf16), preferred_element_type=f32)

            def block(j, _):
                s = scores_of(j)
                old = m_buf[...]
                m = jnp.maximum(old, jnp.max(s, axis=0, keepdims=True))
                weights = jnp.exp(s - m)
                scale = jnp.exp(old - m)
                l_buf[...] = l_buf[...] * scale + jnp.sum(weights, axis=0, keepdims=True)
                m_buf[...] = m
                acc[...] = acc[...] * scale + jnp.dot(
                    vt_buf[j], weights.astype(bf16), preferred_element_type=f32)
                return 0

            lax.fori_loop(0, e, block, 0)
            a = (acc[...] / l_buf[...]).T
            diff = a[:sub] - lam * a[sub:]
            inverse = lax.rsqrt(jnp.mean(diff * diff, axis=-1, keepdims=True) + norm_eps)
            hn_send[e] = (diff * inverse * gain).astype(bf16)

            @pl.when(e != me)
            def _():
                hn_copy(e).start()

            return 0

        lax.fori_loop(0, g, member, 0)

        @pl.when(p == 0)
        def _():
            for step in range(1, n):
                tok_arrival(lax.rem(me + step, n)).wait_recv()
            for step in range(1, n_tp):
                tok_spread(lax.rem(my_tp + step, n_tp)).start()

        return 0

    def hn_copy(dest):
        return pltpu.make_async_remote_copy(
            hn_send.at[dest], hn_buf.at[me], h_ss.at[dest], h_rs.at[me],
            device_id={"ep": dest}, device_id_type=MESH)

    lax.fori_loop(0, heads, group, 0)
    hn_buf[me] = hn_send[me]
    for step in range(1, n):
        source = lax.rem(me + step, n)
        recv(hn_buf, h_rs, source).wait_recv()
    w_copy.wait()
    for part in range(g):
        normed = jnp.concatenate(
            [hn_buf[h * g + lax.rem(part + me, g)] for h in range(heads)], axis=1)
        for t in range(n_tp):
            piece = out_ref.shape[2]
            out_ref[t, part * sub : (part + 1) * sub, :] = jnp.dot(
                normed, w_buf[:, t * piece : (t + 1) * piece], preferred_element_type=f32).astype(bf16)
    for step in range(1, n):
        dest = lax.rem(me + step, n)
        if step % g == 0:
            k_copy(dest).wait_send()
            v_copy(dest).wait_send()
        q_copy(dest).wait_send()
        hn_copy(dest).wait_send()
        tok_copy(dest).wait_send()
    for step in range(1, n_tp):
        other = lax.rem(my_tp + step, n_tp)
        spread_arrival(other).wait_recv()
        tok_spread(other).wait_send()
    for p in range(heads):
        for step in range(1, g):
            for copy in forward(p * g + my_core, step):
                copy.wait_send()


def g_cols(sub):
    return 2 * sub


def exchange_attention(query_pairs, key_pairs, value_rows, head_lambda, head_gain, out_weight, outgoing):
    n = lax.axis_size("ep")
    rows = query_pairs.shape[0]
    heads = head_lambda.shape[0]
    width = query_pairs.shape[1] // heads
    head_size = width // 2
    vw = value_rows.shape[1] // heads
    sub = rows * heads // n
    positions = lax.axis_index("ep") * rows + jnp.arange(rows, dtype=jnp.int32)
    half = head_size // 2
    frequency = theta_base ** (-(jnp.arange(half, dtype=f32) * 2.0) / head_size)
    angles = positions.astype(f32)[:, None] * frequency[None, :]
    cosine, sine = jnp.cos(angles), jnp.sin(angles)
    cosines = jnp.concatenate([cosine] * 4, axis=1)
    sines = jnp.concatenate([-sine, sine] * 2, axis=1)
    turned = jax.ShapeDtypeStruct((heads, rows, width), bf16)
    rq, rk = pl.pallas_call(
        functools.partial(rotate_kernel, head_size, head_size ** (-0.5)),
        out_shape=(turned, turned),
        name="rotate",
    )(query_pairs, key_pairs, cosines, sines)
    any_spec = pl.BlockSpec(memory_space=pl.ANY)
    vmem = pl.BlockSpec(memory_space=pltpu.VMEM)
    dma = pltpu.SemaphoreType.DMA
    g = n // heads
    n_tp = lax.axis_size("tp")
    return pl.pallas_call(
        functools.partial(attention_kernel, n, heads),
        out_shape=(
            jax.ShapeDtypeStruct((n_tp, rows, out_weight.shape[1] // n_tp), bf16),
            jax.ShapeDtypeStruct((n_tp,) + outgoing.shape, bf16),
        ),
        in_specs=[pl.BlockSpec(memory_space=pltpu.SMEM), vmem] + [any_spec] * 5,
        out_specs=(vmem, any_spec),
        scratch_shapes=[
            pltpu.VMEM((n, sub, width), bf16),
            pltpu.VMEM((n, rows, width), bf16),
            pltpu.VMEM((n, rows, vw), bf16),
            pltpu.VMEM((n, vw, rows), bf16),
            pltpu.VMEM((n, sub, vw), bf16),
            pltpu.VMEM((n, sub, vw), bf16),
            pltpu.VMEM(out_weight.shape, bf16),
            pltpu.VMEM((vw, 2 * sub), f32),
            pltpu.VMEM((1, 2 * sub), f32),
            pltpu.VMEM((1, 2 * sub), f32),
            dma((n,)), dma((n,)), dma((n,)), dma((n,)), dma((n,)), dma((n,)),
            dma((n, g)), dma((n,)), dma((n, g)), dma((n,)),
            dma((n,)), dma((n,)), dma((4,)), dma(()),
            dma((n,)), dma((n,)), dma((n_tp,)), dma((n_tp,)),
        ],
        compiler_params=pltpu.CompilerParams(
            collective_id=0, has_side_effects=True, vmem_limit_bytes=56 * 2**20),
        cost_estimate=pl.CostEstimate(flops=20 * 10**9, bytes_accessed=8 * 2**20, transcendentals=5 * 10**6),
        name="attention",
    )(head_lambda, head_gain.reshape(1, vw), rq, rk, value_rows, out_weight, outgoing)


def expert_kernel(
    n, n_tp, mix_ref, arr_ref, xn_ref, place_ref, rw_ref, wg_ref, wu_ref, wd_ref, sg_ref, su_ref, sd_ref,
    attn_ref, moe_ref,
    mix_in, arr, wg, wu, wd, sg, su, sd, sh_send, sh_in, ex_send, ex_in, y_buf, ret,
    loc, m_ss, m_rs, s_ss, s_rs, e_ss, e_rs, y_ss, y_rs,
):
    me = lax.axis_index("ep")
    my_tp = lax.axis_index("tp")
    piece = moe_ref.shape[1]
    cap = y_buf.shape[1]
    barrier = pltpu.get_barrier_semaphore()
    for step in range(1, n):
        pl.semaphore_signal(barrier, inc=1, device_id={"ep": lax.rem(me + step, n)}, device_id_type=MESH)
    for step in range(1, n_tp):
        pl.semaphore_signal(barrier, inc=1, device_id={"tp": lax.rem(my_tp + step, n_tp)}, device_id_type=MESH)
    loads = [
        pltpu.make_async_copy(source, target, loc.at[i])
        for i, (source, target) in enumerate((
            (sg_ref, sg), (su_ref, su), (sd_ref, sd), (arr_ref, arr),
            (wg_ref.at[0], wg), (wu_ref.at[0], wu), (wd_ref.at[0], wd),
            (mix_ref.at[my_tp], mix_in.at[my_tp])))
    ]
    for load in loads:
        load.start()
    pl.semaphore_wait(barrier, n - 1 + n_tp - 1)

    def scatter(send, into, send_sems, recv_sems, dest):
        return pltpu.make_async_remote_copy(
            send.at[dest], into.at[my_tp], send_sems.at[dest], recv_sems.at[my_tp],
            device_id={"tp": dest}, device_id_type=MESH)

    def arrival(into, recv_sems, source, axis):
        return pltpu.make_async_remote_copy(
            into.at[source], into.at[source], recv_sems.at[source], recv_sems.at[source],
            device_id={axis: lax.rem(lax.axis_index(axis) + 1, n if axis == "ep" else n_tp)},
            device_id_type=MESH)

    peers = [lax.rem(my_tp + step, n_tp) for step in (*range(1, n_tp), 0)]
    for dest in peers[:-1]:
        scatter(mix_ref, mix_in, m_ss, m_rs, dest).start()

    def columns(dest):
        return pl.ds(pl.multiple_of(dest * piece, piece), piece)

    def gated(gate, up):
        return (gate / (1.0 + jnp.exp(-gate)) * up).astype(bf16)

    for i in (0, 1, 2):
        loads[i].wait()
    xn = xn_ref[...]
    hidden = gated(
        jnp.dot(xn, sg[...], preferred_element_type=f32),
        jnp.dot(xn, su[...], preferred_element_type=f32))
    for dest in peers:
        sh_send[dest] = jnp.dot(hidden, sd[:, columns(dest)], preferred_element_type=f32).astype(bf16)
    for i in (3, 4, 5, 6):
        loads[i].wait()
    gate = up = None
    for t in range(n_tp):
        rows = arr[t].reshape(n * cap, piece)
        span = slice(t * piece, (t + 1) * piece)
        gate_part = jnp.dot(rows, wg[span, :], preferred_element_type=f32)
        up_part = jnp.dot(rows, wu[span, :], preferred_element_type=f32)
        gate = gate_part if gate is None else gate + gate_part
        up = up_part if up is None else up + up_part
    hidden = gated(gate, up)
    for dest in peers:
        ex_send[dest] = jnp.dot(hidden, wd[:, columns(dest)], preferred_element_type=f32).astype(bf16)
        if dest is not peers[-1]:
            scatter(ex_send, ex_in, e_ss, e_rs, dest).start()
    for dest in peers[:-1]:
        scatter(sh_send, sh_in, s_ss, s_rs, dest).start()
    loads[7].wait()
    for source in peers[:-1]:
        arrival(mix_in, m_rs, source, "tp").wait_recv()
    total = mix_in[0].astype(f32)
    for t in range(1, n_tp):
        total = total + mix_in[t].astype(f32)
    attn_ref[...] = total.astype(bf16)

    def y_copy(dest):
        return pltpu.make_async_remote_copy(
            y_buf.at[dest], ret.at[me], y_ss.at[dest], y_rs.at[me],
            device_id={"ep": dest}, device_id_type=MESH)

    y = ex_send[my_tp].astype(f32)
    for source in peers[:-1]:
        arrival(ex_in, e_rs, source, "tp").wait_recv()
        y = y + ex_in[source].astype(f32)
    y_buf[...] = y.astype(bf16).reshape(n, cap, piece)
    for step in range(1, n):
        y_copy(lax.rem(me + step, n)).start()
    ret[me] = y_buf[me]
    out = sh_send[my_tp].astype(f32)
    for source in peers[:-1]:
        arrival(sh_in, s_rs, source, "tp").wait_recv()
        out = out + sh_in[source].astype(f32)
    for step in range(1, n):
        arrival(ret, y_rs, lax.rem(me + step, n), "ep").wait_recv()
    returned = ret[...].reshape(n * cap, piece)
    for k in range(place_ref.shape[0]):
        out = out + rw_ref[:, k : k + 1] * jnp.dot(place_ref[k], returned, preferred_element_type=f32)
    moe_ref[...] = out.astype(bf16)
    for dest in peers[:-1]:
        scatter(mix_ref, mix_in, m_ss, m_rs, dest).wait_send()
        scatter(ex_send, ex_in, e_ss, e_rs, dest).wait_send()
        scatter(sh_send, sh_in, s_ss, s_rs, dest).wait_send()
    for step in range(1, n):
        y_copy(lax.rem(me + step, n)).wait_send()


def exchange_all(
    query_pairs, key_pairs, value_rows, head_lambda, head_gain, out_weight, normed, routes, route_weight,
    gate_weight, up_weight, down_weight, shared_gate, shared_up, shared_down,
):
    n, n_tp = lax.axis_size("ep"), lax.axis_size("tp")
    tokens, model = normed.shape
    piece = model // n_tp
    rows = query_pairs.shape[0]
    cap = -(-(tokens * TOP_K * 5 // (4 * n)) // 8) * 8
    onehot = (routes[:, :, None] == jnp.arange(n, dtype=jnp.int32)).astype(bf16)
    lower = jnp.tril(jnp.ones((tokens, tokens), bf16))
    ranks = jnp.dot(lower, jnp.sum(onehot, axis=1), preferred_element_type=f32) - 1.0
    slots = jnp.sum(onehot.astype(f32) * (ranks[:, None, :] + jnp.arange(n, dtype=f32) * cap), axis=-1)
    slots = slots.astype(jnp.int32).T
    place = (slots[:, :, None] == jnp.arange(n * cap, dtype=jnp.int32)).astype(bf16)
    part = lax.dynamic_slice_in_dim(normed, lax.axis_index("tp") * piece, piece, axis=1)
    outgoing = lax.dot_general(
        jnp.sum(place, axis=0), part, (((0,), (0,)), ((), ())), preferred_element_type=f32).astype(bf16)
    mix, arr = exchange_attention(
        query_pairs, key_pairs, value_rows, head_lambda, head_gain, out_weight, outgoing.reshape(n, cap, piece))
    any_spec = pl.BlockSpec(memory_space=pl.ANY)
    vmem = pl.BlockSpec(memory_space=pltpu.VMEM)
    dma = pltpu.SemaphoreType.DMA
    hidden, shared = gate_weight.shape[2], shared_gate.shape[1]
    return pl.pallas_call(
        functools.partial(expert_kernel, n, n_tp),
        out_shape=(
            jax.ShapeDtypeStruct((rows, piece), bf16),
            jax.ShapeDtypeStruct((tokens, piece), bf16),
        ),
        in_specs=[any_spec, any_spec, vmem, vmem, vmem] + [any_spec] * 6,
        out_specs=(vmem, vmem),
        scratch_shapes=[
            pltpu.VMEM((n_tp, rows, piece), bf16),
            pltpu.VMEM((n_tp, n, cap, piece), bf16),
            pltpu.VMEM((model, hidden), bf16),
            pltpu.VMEM((model, hidden), bf16),
            pltpu.VMEM((hidden, model), bf16),
            pltpu.VMEM((model, shared), bf16),
            pltpu.VMEM((model, shared), bf16),
            pltpu.VMEM((shared, model), bf16),
            pltpu.VMEM((n_tp, tokens, piece), bf16),
            pltpu.VMEM((n_tp, tokens, piece), bf16),
            pltpu.VMEM((n_tp, n * cap, piece), bf16),
            pltpu.VMEM((n_tp, n * cap, piece), bf16),
            pltpu.VMEM((n, cap, piece), bf16),
            pltpu.VMEM((n, cap, piece), bf16),
            dma((8,)), dma((n_tp,)), dma((n_tp,)), dma((n_tp,)), dma((n_tp,)), dma((n_tp,)), dma((n_tp,)),
            dma((n,)), dma((n,)),
        ],
        compiler_params=pltpu.CompilerParams(
            collective_id=1, has_side_effects=True, vmem_limit_bytes=60 * 2**20),
        cost_estimate=pl.CostEstimate(flops=10 * 10**9, bytes_accessed=16 * 2**20, transcendentals=5 * 10**5),
        name="experts",
    )(mix, arr, normed, place, route_weight, gate_weight, up_weight, down_weight, shared_gate, shared_up, shared_down)


def local(
    query_pairs,
    key_pairs,
    value_rows,
    head_lambda,
    head_gain,
    out_weight,
    moe_input,
    ffn_gain,
    routes,
    route_weight,
    gate_weight,
    up_weight,
    down_weight,
    shared_gate,
    shared_up,
    shared_down,
):
    n = lax.axis_size("ep")
    heads = head_lambda.shape[0]
    rows = query_pairs.shape[0]
    fits = n % heads == 0 and n // heads > 1 and (rows * heads) % (n * 64) == 0
    row_values = moe_input.astype(jnp.float32)
    inverse_norm = lax.rsqrt(jnp.mean(row_values * row_values, axis=-1, keepdims=True) + norm_eps)
    normed = (row_values * inverse_norm * ffn_gain).astype(jnp.bfloat16)
    if fits:
        return exchange_all(
            query_pairs, key_pairs, value_rows, head_lambda, head_gain, out_weight, normed, routes, route_weight,
            gate_weight, up_weight, down_weight, shared_gate, shared_up, shared_down,
        )
    attn_out = generic_attention(query_pairs, key_pairs, value_rows, head_lambda, head_gain, out_weight)
    token_rows = normed.shape[0]
    experts = lax.axis_size("ep")
    capacity = token_rows * TOP_K * 5 // (4 * experts)
    flat_routes = routes.reshape(-1)
    onehot = (flat_routes[:, None] == jnp.arange(experts, dtype=jnp.int32)).astype(jnp.int32)
    slot_rank = jnp.sum((jnp.cumsum(onehot, axis=0) - 1) * onehot, axis=-1)
    slot_index = flat_routes * capacity + slot_rank
    token_index = jnp.arange(token_rows * TOP_K, dtype=jnp.int32) // TOP_K
    slot_rows = (
        jnp.full((experts * capacity,), token_rows, jnp.int32).at[slot_index].set(token_index)
    )
    padded = jnp.concatenate([normed, jnp.zeros((1, normed.shape[1]), jnp.bfloat16)], axis=0)
    outgoing = padded[slot_rows]
    arrived = lax.all_to_all(outgoing, "ep", split_axis=0, concat_axis=0, tiled=True)
    gate_part = jnp.dot(arrived, gate_weight[0], preferred_element_type=jnp.float32)
    up_part = jnp.dot(arrived, up_weight[0], preferred_element_type=jnp.float32)
    hidden = (jax.nn.silu(gate_part) * up_part).astype(jnp.bfloat16)
    expert_terms = jnp.dot(hidden, down_weight[0], preferred_element_type=jnp.float32)
    shared_gated = jnp.dot(normed, shared_gate, preferred_element_type=jnp.float32)
    shared_lifted = jnp.dot(normed, shared_up, preferred_element_type=jnp.float32)
    shared_hidden = (jax.nn.silu(shared_gated) * shared_lifted).astype(jnp.bfloat16)
    shared_terms = jnp.dot(shared_hidden, shared_down, preferred_element_type=jnp.float32)
    expert_sum, shared_sum = (
        lax.psum_scatter(
            expert_terms.astype(jnp.bfloat16), "tp", scatter_dimension=1, tiled=True
        ).astype(jnp.float32),
        lax.psum_scatter(
            shared_terms.astype(jnp.bfloat16), "tp", scatter_dimension=1, tiled=True
        ).astype(jnp.float32),
    )
    returned = lax.all_to_all(
        expert_sum.astype(jnp.bfloat16), "ep", split_axis=0, concat_axis=0, tiled=True
    )
    picked = returned[slot_index.reshape(token_rows, TOP_K)]
    moe_out = (
        jnp.sum(route_weight[..., None] * picked.astype(jnp.float32), axis=1) + shared_sum
    ).astype(jnp.bfloat16)
    return (attn_out, moe_out)


def solution(mesh):
    return jax.shard_map(
        local,
        mesh=mesh,
        in_specs=(
            P("ep", "tp"),
            P("ep", "tp"),
            P("ep", "tp"),
            P("tp"),
            P(),
            P("tp", None),
            P("ep", None),
            P(),
            P("ep", None),
            P("ep", None),
            P("ep", None, "tp"),
            P("ep", None, "tp"),
            P("ep", "tp", None),
            P(None, "tp"),
            P(None, "tp"),
            P("tp", None),
        ),
        out_specs=(P("ep", "tp"), P("ep", "tp")),
        check_vma=False,
    )
```

profile of v0, /device:TPU:17, one launch (start us, length us, event | category | flops | bytes accessed | tf_op | source)
XLA Modules:
  0.0 134.6 jit_solution(16845973564310978378)
XLA Ops:
  0.6 0.0 copy-start
  0.6 0.0 copy-start.2
  0.7 0.8 fusion.9
  1.5 0.0 copy-start.3
  1.5 1.1 pad_maximum_fusion
  2.6 2.6 %rotate.1 = (bf16[4,384,128]{2,1,0:T(8,128)(2,1)}, bf16[4,384,128]{2,1,0:T(8,128)(2,1)}) custom-call(bf16[384,512]{1,0:T(8,128)(2,1)} %q_ref.1, bf16[384,512]{1,0:T(8,128)(2,1)} %k_ref.1, f32[384,128]{1,0:T(8,128)} %get-tuple-element.13.cos_ref, f32[384,128]{1,0:T(8,128)} %get-tuple-element.14.sin_ref), custom_call_target="tpu_custom_call" | custom-call | tf_op jit(solution)/shard_map/rotate/pallas_call | solution.py:370
  5.2 0.0 copy-done
  5.2 0.2 fusion
  5.4 0.0 copy-done.2
  5.4 0.2 fusion.2.xn_ref
  5.6 0.0 copy-done.3
  5.7 0.0 copy-start.1
  5.7 0.1 fusion.3
  5.8 0.1 multiply_reduce_fusion
  5.9 0.1 fusion.7
  6.0 1.1 convolution_convert_fusion
  7.1 0.0 copy-start.4
  7.1 61.6 %attention.1 = (bf16[4,384,512]{2,1,0:T(8,128)(2,1)}, bf16[4,8,56,512]{3,2,1,0:T(8,128)(2,1)}) custom-call(f32[4]{0:T(128)} %lam_ref.1, f32[1,128]{1,0:T(1,128)} %bitcast.7, bf16[4,384,128]{2,1,0:T(8,128)(2,1)} %get-tuple-element.6.rq_ref, bf16[4,384,128]{2,1,0:T(8,128)(2,1)} %get-tuple-element.7.rk_ref, bf16[384,512]{1,0:T(8,128)(2,1)} %v_ref.1, ...), custom_call_target="tpu_custom_call" | custom-call | flops 20000000000 | bytes 8388608 | tf_op jit(solution)/shard_map/attention/pallas_call | solution.py:380
  68.7 0.0 copy-done.1
  68.7 0.8 fusion.4.place_ref
  69.6 0.0 copy-done.4
  69.6 0.8 copy.23.rw_ref
  70.3 60.9 %experts.1 = (bf16[384,512]{1,0:T(8,128)(2,1)}, bf16[160,512]{1,0:T(8,128)(2,1)}) custom-call(bf16[4,384,512]{2,1,0:T(8,128)(2,1)} %get-tuple-element.8.mix_ref, bf16[4,8,56,512]{3,2,1,0:T(8,128)(2,1)} %get-tuple-element.9.arr_ref, bf16[160,2048]{1,0:T(8,128)(2,1)} %copy-done.1, bf16[2,160,448]{2,1,0:T(8,128)(2,1)} %fusion.4.place_ref, ...), custom_call_target="tpu_custom_call" | custom-call | flops 10000000000 | bytes 16777216 | tf_op jit(solution)/shard_map/experts/pallas_call | solution.py:546
  131.2 1.8 %copy.26 = bf16[384,512]{1,0:T(8,128)(2,1)} copy(bf16[384,512]{1,0:T(8,128)(2,1)} %get-tuple-element.17) | data formatting | bytes 786432
  133.0 1.6 %copy.27 = bf16[160,512]{1,0:T(8,128)(2,1)} copy(bf16[160,512]{1,0:T(8,128)(2,1)} %get-tuple-element.18) | data formatting | bytes 327680
  (6 shorter events, 0.0 us)
Async XLA Ops:
  0.6 4.6 %copy-start = (bf16[160,2048]{1,0:T(8,128)(2,1)S(1)}, bf16[160,2048]{1,0:T(8,128)(2,1)}, u32[]{:S(2)}) copy-start(bf16[160,2048]{1,0:T(8,128)(2,1)} %param.22) | copy-start | bytes 1966084
  0.6 4.8 %copy-start.2 = (f32[2048]{0:T(1024)S(1)}, f32[2048]{0:T(1024)}, u32[]{:S(2)}) copy-start(f32[2048]{0:T(1024)} %param.23) | copy-start | bytes 24580
  1.5 4.2 %copy-start.3 = (s32[160,2]{0,1:T(2,128)S(1)}, s32[160,2]{0,1:T(2,128)}, u32[]{:S(2)}) copy-start(s32[160,2]{0,1:T(2,128)} %param.24) | copy-start | bytes 3844
  5.7 63.1 %copy-start.1 = (bf16[160,2048]{1,0:T(8,128)(2,1)}, bf16[160,2048]{1,0:T(8,128)(2,1)S(1)}, u32[]{:S(2)}) copy-start(bf16[160,2048]{1,0:T(8,128)(2,1)S(1)} %fusion.2.xn_ref) | copy-start | bytes 1966084
  7.1 62.5 %copy-start.4 = (f32[160,2]{0,1:T(2,128)S(1)}, f32[160,2]{0,1:T(2,128)}, u32[]{:S(2)}) copy-start(f32[160,2]{0,1:T(2,128)} %param.25) | copy-start | bytes 3844
where the time goes:
time: 137 us; the launch traced here: 135 us
  Pallas kernels  125 us (91%)
  local copies, waits for them, and re-layouts  4.14 us (3%)
  other arithmetic  3.4 us (2%)
    pallas_call x1, Pallas kernels, exchange_attention(): pl.pallas_call(functools.partial(attention_kernel, n, heads), out_shape=(...  61.6 us
    pallas_call x1, Pallas kernels, exchange_all(): pl.pallas_call(functools.partial(expert_kernel, n, n_tp), out_shape=(jax....  60.9 us
    unnamed x13, local copies, waits for them, and re-layouts  4.14 us

commit v1 on v0

v1 whole, which is shorter than its diff:
```python
import functools

import jax
import jax.numpy as jnp
import numpy as np
from jax import lax
from jax.experimental import pallas as pl
from jax.experimental.pallas import tpu as pltpu
from jax.sharding import PartitionSpec as P

TOP_K = 2
KEY_BLOCK = 128


theta_base = 500000.0
norm_eps = 1e-06
masked_low = -1e30


def rotate(inputs, positions):
    half_size = inputs.shape[-1] // 2
    frequency = theta_base ** (-(jnp.arange(half_size, dtype=jnp.float32) * 2.0) / inputs.shape[-1])
    angles = positions.astype(jnp.float32)[:, None] * frequency[None, :]
    cosine = jnp.cos(angles)[:, None, None, :]
    sine_part = jnp.sin(angles)[:, None, None, :]
    front_half = inputs[..., :half_size]
    back_half = inputs[..., half_size:]
    return jnp.concatenate(
        [front_half * cosine - back_half * sine_part, back_half * cosine + front_half * sine_part],
        axis=-1,
    )


def generic_attention(query_pairs, key_pairs, value_rows, head_lambda, head_gain, out_weight):
    local_rows = query_pairs.shape[0]
    local_heads = head_lambda.shape[0]
    head_size = query_pairs.shape[1] // (2 * local_heads)
    value_size = value_rows.shape[1] // local_heads
    positions = lax.axis_index("ep") * local_rows + jnp.arange(local_rows, dtype=jnp.int32)
    rot_queries = rotate(
        query_pairs.astype(jnp.float32).reshape(local_rows, local_heads, 2, head_size), positions
    ).astype(jnp.bfloat16)
    rot_keys = rotate(
        key_pairs.astype(jnp.float32).reshape(local_rows, local_heads, 2, head_size), positions
    ).astype(jnp.bfloat16)
    rot_keys = rot_keys.reshape(local_rows, local_heads * 2 * head_size)
    zero_init = (
        jnp.full((local_heads, 2, local_rows), masked_low, jnp.float32),
        jnp.zeros((local_heads, 2, local_rows), jnp.float32),
        jnp.zeros((local_heads, 2, local_rows, value_size), jnp.float32),
    )
    piece_keys = lax.all_gather(rot_keys, "ep", axis=0, tiled=True)
    piece_values = lax.all_gather(value_rows, "ep", axis=0, tiled=True)
    block_count = piece_keys.shape[0] // KEY_BLOCK
    group_size = 4
    group_count = block_count // group_size
    grouped_keys = piece_keys.reshape(group_count, group_size, KEY_BLOCK, local_heads, 2, head_size)
    grouped_values = piece_values.reshape(
        group_count, group_size, KEY_BLOCK, local_heads, value_size
    )

    def one_group(current, inputs):
        block_keys, block_values, group_index = inputs
        key_positions = group_index * group_size * KEY_BLOCK + jnp.arange(
            group_size * KEY_BLOCK, dtype=jnp.int32
        ).reshape(group_size, KEY_BLOCK)
        scores = jnp.einsum(
            "qhmd,gkhmd->hmqgk", rot_queries, block_keys, preferred_element_type=jnp.float32
        ) * head_size ** (-0.5)
        allowed = key_positions[None, :, :] <= positions[:, None, None]
        scores = jnp.where(allowed, scores, masked_low)
        block_max = jnp.max(scores, axis=-1)
        weights = jnp.where(allowed, jnp.exp(scores - block_max[..., None]), 0.0)
        block_sum = jnp.sum(weights, axis=-1)
        block_out = jnp.einsum(
            "hmqgk,gkhc->hmqgc",
            weights.astype(jnp.bfloat16),
            block_values,
            preferred_element_type=jnp.float32,
        )
        run_max, run_sum, run_out = current
        new_max = jnp.maximum(run_max, jnp.max(block_max, axis=-1))
        old_scale = jnp.exp(run_max - new_max)
        new_scale = jnp.exp(block_max - new_max[..., None])
        run_sum = run_sum * old_scale + jnp.sum(new_scale * block_sum, axis=-1)
        run_out = run_out * old_scale[..., None] + jnp.sum(
            new_scale[..., None] * block_out, axis=-2
        )
        return ((new_max, run_sum, run_out), None)

    result, _ = lax.scan(
        one_group,
        zero_init,
        (grouped_keys, grouped_values, jnp.arange(group_count, dtype=jnp.int32)),
    )
    run_max, run_sum, run_out = result
    map_outputs = run_out / run_sum[..., None]
    difference = map_outputs[:, 0] - head_lambda[:, None, None] * map_outputs[:, 1]
    inverse_rms = lax.rsqrt(jnp.mean(difference * difference, axis=-1, keepdims=True) + norm_eps)
    normed_heads = (difference * inverse_rms * head_gain).astype(jnp.bfloat16)
    head_rows = normed_heads.transpose(1, 0, 2).reshape(local_rows, local_heads * value_size)
    mixer_terms = jnp.dot(head_rows, out_weight, preferred_element_type=jnp.float32)
    attn_out = lax.psum_scatter(
        mixer_terms.astype(jnp.bfloat16), "tp", scatter_dimension=1, tiled=True
    )
    return attn_out


MESH = pl.DeviceIdType.MESH
f32, bf16 = jnp.float32, jnp.bfloat16


def mega_kernel(
    n, heads, n_tp, head_size, lam_ref, gain_ref, routes_ref, rw_ref, ffn_ref, turn_ref, base_ref,
    q_ref, k_ref, v_ref, x_ref, w_ref, wg_ref, wu_ref, wd_ref, sg_ref, su_ref, sd_ref,
    attn_ref, moe_ref,
    q_in, k_in, v_in, turn, x_in, xn, place, rq, rk, q_buf, k_buf, v_buf, vt_buf, st_buf, acc, m_buf,
    hn_send, hn_buf, w_buf, out_buf, own_buf, arr, wg, wu, wd, sg, su, sd,
    sh_send, sh_in, ex_send, ex_in, mix_send, mix_in, y_buf, ret, rw_pad,
    load, load_v, barrier_free, q_ss, q_rs, k_ss, k_rs, v_ss, v_rs, fk_ss, fk_rs, fv_ss, fv_rs, h_ss, h_rs,
    t_ss, t_rs, o_ss, o_rs, x_ss, x_rs, m_ss, m_rs, s_ss, s_rs, e_ss, e_rs, y_ss, y_rs,
):
    me, my_tp = lax.axis_index("ep"), lax.axis_index("tp")
    g = n // heads
    chip, core = me // g, me % g
    rows, width = k_buf.shape[1:]
    vw = v_buf.shape[2]
    sub = rows // g
    cap, piece = out_buf.shape[1:]
    tokens = xn.shape[0]
    top_k = rw_ref.shape[0]
    half = head_size // 2
    side = chip // (heads // 2)

    def mirrored(p):
        return p + side * (heads - 1 - 2 * p)

    near = mirrored(chip)

    def nearest(s):
        return mirrored(jnp.where(s <= near, near - s, s))

    barrier = pltpu.get_barrier_semaphore()
    for step in range(1, n):
        pl.semaphore_signal(barrier, inc=1, device_id={"ep": lax.rem(me + step, n)}, device_id_type=MESH)
    for step in range(1, n_tp):
        pl.semaphore_signal(barrier, inc=1, device_id={"tp": lax.rem(my_tp + step, n_tp)}, device_id_type=MESH)
    loads = [
        pltpu.make_async_copy(source, target, load.at[i])
        for i, (source, target) in enumerate((
            (x_ref, x_in), (turn_ref, turn), (k_ref, k_in), (q_ref, q_in),
            (sg_ref, sg), (su_ref, su), (sd_ref, sd),
            (wg_ref.at[0], wg), (wu_ref.at[0], wu), (wd_ref.at[0], wd), (w_ref, w_buf)))
    ]
    values = [
        pltpu.make_async_copy(v_ref.at[:, h * vw : (h + 1) * vw], v_in.at[h], load_v.at[h]) for h in range(heads)
    ]
    for copy in loads[:4]:
        copy.start()
    for copy in values:
        copy.start()
    for copy in loads[4:]:
        copy.start()

    def to_ep(source, target, send_sem, recv_sem, dest):
        return pltpu.make_async_remote_copy(
            source, target, send_sem, recv_sem, device_id={"ep": dest}, device_id_type=MESH)

    def to_tp(source, target, send_sem, recv_sem, dest):
        return pltpu.make_async_remote_copy(
            source, target, send_sem, recv_sem, device_id={"tp": dest}, device_id_type=MESH)

    def arrived(ref, sem):
        to_ep(ref, ref, sem, sem, lax.rem(me + 1, n)).wait_recv()

    peers = [lax.rem(my_tp + step, n_tp) for step in (*range(1, n_tp), 0)]

    def columns(t):
        return pl.ds(pl.multiple_of(t * piece, piece), piece)

    expert = lax.broadcasted_iota(jnp.int32, (n, tokens), 0)
    chosen = [(routes_ref[k : k + 1, :] == expert).astype(f32) for k in range(top_k)]
    earlier = lax.broadcasted_iota(jnp.int32, (tokens, tokens), 0) <= lax.broadcasted_iota(jnp.int32, (tokens, tokens), 1)
    ranks = jnp.dot(sum(chosen).astype(bf16), earlier.astype(bf16), preferred_element_type=f32) - 1.0
    slot = ranks + (expert * cap).astype(f32)
    slots = [jnp.sum(c * slot, axis=0, keepdims=True) for c in chosen]
    slot_row = lax.broadcasted_iota(jnp.int32, (n * cap, tokens), 0).astype(f32)
    marks = [(slot_row == s).astype(f32) for s in slots]
    for k in range(top_k):
        place[k] = marks[k].astype(bf16).reshape(n, cap, tokens)
    loads[0].wait()
    x = x_in[...].astype(f32)
    inverse = lax.rsqrt(jnp.mean(x * x, axis=-1, keepdims=True) + norm_eps)
    xn[...] = (x * inverse * ffn_ref[...]).astype(bf16)
    out_buf[...] = jnp.dot(
        sum(marks).astype(bf16), xn[:, columns(my_tp)], preferred_element_type=f32).astype(bf16).reshape(n, cap, piece)

    def own_rows(dest):
        mark = place[0, dest]
        for k in range(1, top_k):
            mark = mark + place[k, dest]
        return jnp.dot(mark, xn[...], preferred_element_type=f32).astype(bf16)

    pl.semaphore_wait(barrier, n - 1 + n_tp - 1)

    def tok_copy(dest):
        return to_ep(out_buf.at[dest], arr.at[my_tp, me], t_ss.at[dest], t_rs.at[me], dest)

    def own_copy(step):
        dest = chip * g + lax.rem(core + step, g)
        return to_ep(own_buf.at[step - 1], arr.at[:, me], o_ss.at[step - 1], o_rs.at[me], dest)

    for s in range(1, heads):
        for c in range(g):
            tok_copy(nearest(s) * g + c).start()
    for step in range(g):
        full = own_rows(chip * g + lax.rem(core + step, g))
        for t in range(n_tp):
            part = full[:, t * piece : (t + 1) * piece]
            if step == 0:
                arr[t, me] = part
            else:
                own_buf[step - 1, t] = part
        if step:
            own_copy(step).start()

    base_cos, base_sin = base_ref[0, pl.ds(me, 1)], base_ref[1, pl.ds(me, 1)]
    lane = lax.broadcasted_iota(jnp.int32, (1, width), 1)
    front = lane % head_size < half
    loads[1].wait()
    cosine = turn[0] * base_cos - turn[1] * base_sin
    sine = turn[1] * base_cos + turn[0] * base_sin
    sine = jnp.where(front, -sine, sine)

    def turned(source, h):
        x = source[:, h * width : (h + 1) * width].astype(f32)
        partner = jnp.where(front, pltpu.roll(x, width - half, 1), pltpu.roll(x, half, 1))
        return (x * cosine + partner * sine).astype(bf16)

    loads[2].wait()
    for h in range(heads):
        rk[h] = turned(k_in, h)
    loads[3].wait()
    for h in range(heads):
        rq[h] = turned(q_in, h) * jnp.asarray(head_size ** -0.5, bf16)
    for copy in values:
        copy.wait()

    def q_rows(dest):
        return pl.ds(pl.multiple_of(((dest % g + me) % g) * sub, sub), sub)

    def q_copy(dest):
        return to_ep(rq.at[dest // g, q_rows(dest)], q_buf.at[me], q_ss.at[dest], q_rs.at[me], dest)

    def k_copy(dest):
        return to_ep(rk.at[dest // g], k_buf.at[me], k_ss.at[dest], k_rs.at[me], dest)

    def v_copy(dest):
        return to_ep(v_in.at[dest // g], v_buf.at[me], v_ss.at[dest], v_rs.at[me], dest)

    for s in range(1, heads):
        dest = nearest(s) * g + core
        k_copy(dest).start()
        for c in range(g):
            q_copy(nearest(s) * g + c).start()
        v_copy(dest).start()
    for step in range(1, g):
        q_copy(chip * g + lax.rem(core + step, g)).start()
    q_buf[me] = rq[chip, q_rows(me)]
    k_buf[me] = rk[chip]
    v_buf[me] = v_in[chip]

    def gated(gate, up):
        return (gate / (1.0 + jnp.exp(-gate)) * up).astype(bf16)

    for i in (4, 5, 6):
        loads[i].wait()
    hidden = gated(
        jnp.dot(xn[...], sg[...], preferred_element_type=f32), jnp.dot(xn[...], su[...], preferred_element_type=f32))

    def sh_copy(dest):
        return to_tp(sh_send.at[dest], sh_in.at[my_tp], s_ss.at[dest], s_rs.at[my_tp], dest)

    for dest in peers:
        sh_send[dest] = jnp.dot(hidden, sd[:, columns(dest)], preferred_element_type=f32).astype(bf16)
        if dest is not peers[-1]:
            sh_copy(dest).start()

    lam = lam_ref[chip]
    gain = gain_ref[...]
    vt_rows = vt_buf.shape[1]
    keys = g * rows
    lane_row = lax.broadcasted_iota(jnp.int32, (sub, width), 1)

    def forward(source, step):
        to = chip * g + lax.rem(core + step, g)
        return (
            to_ep(k_buf.at[source], k_buf.at[source], fk_ss.at[source, step], fk_rs.at[source], to),
            to_ep(v_buf.at[source], v_buf.at[source], fv_ss.at[source, step], fv_rs.at[source], to),
        )

    def receive(p):
        direct = p * g + core

        @pl.when(direct != me)
        def _():
            arrived(k_buf.at[direct], k_rs.at[direct])
            arrived(v_buf.at[direct], v_rs.at[direct])

        for step in range(1, g):
            for copy in forward(direct, step):
                copy.start()
        for c in range(g):
            e = p * g + c

            @pl.when(e != me)
            def _():
                arrived(q_buf.at[e], q_rs.at[e])

            q = q_buf[e]
            zero = jnp.zeros_like(q)
            st_buf[p, 2 * c * sub : (2 * c + 1) * sub] = jnp.where(lane_row < width // 2, q, zero)
            st_buf[p, (2 * c + 1) * sub : (2 * c + 2) * sub] = jnp.where(lane_row < width // 2, zero, q)
        for step in range(1, g):
            other = p * g + lax.rem(core + step, g)
            arrived(k_buf.at[other], fk_rs.at[other])
            arrived(v_buf.at[other], fv_rs.at[other])
        for c in range(g):
            vt_buf[p, :vw, c * rows : (c + 1) * rows] = v_buf[p * g + c].astype(f32).T.astype(bf16)
        vt_buf[p, vw:] = jnp.ones((vt_rows - vw, keys), bf16)
        m_buf[p] = jnp.full((1, keys), masked_low, f32)
        acc[p] = jnp.zeros((vt_rows, keys), f32)

    def tile(p, j, diagonal):
        for c in range(g):
            first = c * rows if diagonal else 0
            span = slice(first, keys)
            size = keys - first
            s = lax.dot_general(
                k_buf[j * g + c], st_buf[p, span], (((1,), (1,)), ((), ())), preferred_element_type=f32)
            if diagonal:
                key = lax.broadcasted_iota(jnp.int32, (rows, size), 0) + c * rows
                column = lax.broadcasted_iota(jnp.int32, (rows, size), 1) + first
                block = column // rows
                query = block * rows + column % sub + (core + block) % g * sub
                s = jnp.where(key <= query, s, masked_low)
            old = m_buf[p, :, span]
            m = jnp.maximum(old, jnp.max(s, axis=0, keepdims=True))
            weights = jnp.exp(s - m).astype(bf16)
            m_buf[p, :, span] = m
            acc[p, :, span] = acc[p, :, span] * jnp.exp(old - m) + jnp.dot(
                vt_buf[j, :, c * rows : (c + 1) * rows], weights, preferred_element_type=f32)

    def hn_copy(dest):
        return to_ep(hn_send.at[dest], hn_buf.at[me], h_ss.at[dest], h_rs.at[me], dest)

    def finish(p):
        a = (acc[p, :vw] / acc[p, vw : vw + 1]).T
        for c in range(g):
            e = p * g + c
            diff = a[2 * c * sub : (2 * c + 1) * sub] - lam * a[(2 * c + 1) * sub : (2 * c + 2) * sub]
            inverse = lax.rsqrt(jnp.mean(diff * diff, axis=-1, keepdims=True) + norm_eps)
            hn_send[e] = (diff * inverse * gain).astype(bf16)

            @pl.when(e != me)
            def _():
                hn_copy(e).start()

    def turn_of(p):
        p = mirrored(p)
        return jnp.where(p <= near, near - p, p)

    def attend(s):
        receive(nearest(s))

        def queries(p, _):
            def blocks(j, _):
                @pl.when(jnp.maximum(turn_of(p), turn_of(j)) == s)
                def _():
                    tile(p, j, False)

                return 0

            @pl.when(turn_of(p) == s)
            def _():
                tile(p, p, True)

            @pl.when(turn_of(p) <= s)
            def _():
                lax.fori_loop(0, p, blocks, 0)

            last = 0
            for j in range(heads):
                last = jnp.maximum(last, jnp.where(j <= p, turn_of(j), 0))

            @pl.when(last == s)
            def _():
                finish(p)

            return 0

        lax.fori_loop(0, heads, queries, 0)
        return 0

    def spread_copy(p, dest):
        part = arr.at[my_tp, pl.ds(p * g, g)]
        return to_tp(part, part, x_ss.at[p, dest], x_rs.at[my_tp, p], dest)

    def spread(s):
        p = nearest(s)
        for c in range(g):
            arrived(arr.at[my_tp, p * g + c], t_rs.at[p * g + c])
        for dest in peers[:-1]:
            spread_copy(p, dest).start()

    def ex_copy(dest):
        return to_tp(ex_send.at[dest], ex_in.at[my_tp], e_ss.at[dest], e_rs.at[my_tp], dest)

    def routed():
        for step in range(1, g):
            other = chip * g + lax.rem(core + step, g)
            arrived(arr.at[:, other], o_rs.at[other])
        for s in range(1, heads):
            for t in peers[:-1]:
                arrived(arr.at[t, pl.ds(nearest(s) * g, g)], x_rs.at[t, nearest(s)])
        for i in (7, 8, 9):
            loads[i].wait()
        gate = up = None
        for t in range(n_tp):
            block = arr[t].reshape(n * cap, piece)
            span = slice(t * piece, (t + 1) * piece)
            gate_part = jnp.dot(block, wg[span, :], preferred_element_type=f32)
            up_part = jnp.dot(block, wu[span, :], preferred_element_type=f32)
            gate = gate_part if gate is None else gate + gate_part
            up = up_part if up is None else up + up_part
        hidden = gated(gate, up)
        for dest in peers:
            ex_send[dest] = jnp.dot(hidden, wd[:, columns(dest)], preferred_element_type=f32).astype(bf16)
            if dest is not peers[-1]:
                ex_copy(dest).start()

    def phase(s, _):
        attend(s)

        @pl.when(s == 0)
        def _():
            for step in range(1, heads):
                spread(step)

        @pl.when(s == 1)
        def _():
            routed()

        return 0

    lax.fori_loop(0, heads, phase, 0)

    hn_buf[me] = hn_send[me]
    for step in range(1, n):
        source = lax.rem(me + step, n)
        arrived(hn_buf.at[source], h_rs.at[source])
    loads[10].wait()

    def mix_copy(dest):
        return to_tp(mix_send.at[dest], mix_in.at[my_tp], m_ss.at[dest], m_rs.at[my_tp], dest)

    normed = [
        jnp.concatenate([hn_buf[h * g + (part + n - me) % g] for h in range(heads)], axis=1) for part in range(g)]
    for dest in peers:
        for part in range(g):
            mix_send[dest, part * sub : (part + 1) * sub] = jnp.dot(
                normed[part], w_buf[:, columns(dest)], preferred_element_type=f32).astype(bf16)
        if dest is not peers[-1]:
            mix_copy(dest).start()

    def y_copy(dest):
        return to_ep(y_buf.at[dest], ret.at[me], y_ss.at[dest], y_rs.at[me], dest)

    y = ex_send[my_tp].astype(f32)
    for source in peers[:-1]:
        arrived(ex_in.at[source], e_rs.at[source])
        y = y + ex_in[source].astype(f32)
    y_buf[...] = y.astype(bf16).reshape(n, cap, piece)
    for s in range(1, heads):
        for c in range(g):
            y_copy(nearest(s) * g + c).start()
    for step in range(1, g):
        y_copy(chip * g + lax.rem(core + step, g)).start()
    ret[me] = y_buf[me]
    out = sh_send[my_tp].astype(f32)
    for source in peers[:-1]:
        arrived(sh_in.at[source], s_rs.at[source])
        out = out + sh_in[source].astype(f32)
    rw_pad[...] = jnp.zeros_like(rw_pad)
    rw_pad[:top_k, :tokens] = rw_ref[...]
    scale = rw_pad[...].T
    for step in range(1, n):
        source = lax.rem(me + step, n)
        arrived(ret.at[source], y_rs.at[source])
    returned = ret[...].reshape(n * cap, piece)
    for k in range(top_k):
        out = out + scale[:tokens, k : k + 1] * lax.dot_general(
            place[k].reshape(n * cap, tokens), returned, (((0,), (0,)), ((), ())), preferred_element_type=f32)
    moe_ref[...] = out.astype(bf16)

    total = mix_send[my_tp].astype(f32)
    for source in peers[:-1]:
        arrived(mix_in.at[source], m_rs.at[source])
        total = total + mix_in[source].astype(f32)
    attn_ref[...] = total.astype(bf16)

    for s in range(1, heads):
        p = nearest(s)
        k_copy(p * g + core).wait_send()
        v_copy(p * g + core).wait_send()
        for c in range(g):
            tok_copy(p * g + c).wait_send()
        for dest in peers[:-1]:
            spread_copy(p, dest).wait_send()
    for step in range(1, n):
        dest = lax.rem(me + step, n)
        q_copy(dest).wait_send()
        hn_copy(dest).wait_send()
        y_copy(dest).wait_send()
    for step in range(1, g):
        own_copy(step).wait_send()
    for p in range(heads):
        for step in range(1, g):
            for copy in forward(p * g + core, step):
                copy.wait_send()
    for dest in peers[:-1]:
        sh_copy(dest).wait_send()
        ex_copy(dest).wait_send()
        mix_copy(dest).wait_send()


def turn_tables(rows, n, head_size):
    half = head_size // 2
    frequency = theta_base ** (-(np.arange(half) * 2.0) / head_size)

    def waves(positions):
        angles = np.tile(positions[:, None] * frequency[None, :], (1, 4))
        return np.stack([np.cos(angles), np.sin(angles)]).astype(np.float32)

    return waves(np.arange(rows)), waves(np.arange(n) * rows)


def exchange_all(
    query_pairs, key_pairs, value_rows, head_lambda, head_gain, out_weight, moe_input, ffn_gain, routes, route_weight,
    gate_weight, up_weight, down_weight, shared_gate, shared_up, shared_down,
):
    n, n_tp = lax.axis_size("ep"), lax.axis_size("tp")
    tokens, model = moe_input.shape
    piece = model // n_tp
    rows = query_pairs.shape[0]
    heads = head_lambda.shape[0]
    width = query_pairs.shape[1] // heads
    head_size = width // 2
    vw = value_rows.shape[1] // heads
    g = n // heads
    sub = rows // g
    keys = g * rows
    cap = -(-(tokens * TOP_K * 5 // (4 * n)) // 8) * 8
    hidden, shared = gate_weight.shape[2], shared_gate.shape[1]
    turns, bases = turn_tables(rows, n, head_size)
    any_spec = pl.BlockSpec(memory_space=pl.ANY)
    vmem = pl.BlockSpec(memory_space=pltpu.VMEM)
    dma = pltpu.SemaphoreType.DMA
    buffers = [
        (rows, heads * width), (rows, heads * width), (heads, rows, vw), ((2, rows, width), f32),
        (tokens, model), (tokens, model), (TOP_K, n, cap, tokens), (heads, rows, width), (heads, rows, width),
        (n, sub, width), (n, rows, width), (n, rows, vw), (heads, vw + 8, keys), (heads, 2 * rows, width),
        ((heads, vw + 8, keys), f32), ((heads, 1, keys), f32), (n, sub, vw), (n, sub, vw), out_weight.shape,
        (n, cap, piece), (g - 1, n_tp, cap, piece), (n_tp, n, cap, piece),
        (model, hidden), (model, hidden), (hidden, model), (model, shared), (model, shared), (shared, model),
        (n_tp, tokens, piece), (n_tp, tokens, piece), (n_tp, n * cap, piece), (n_tp, n * cap, piece),
        (n_tp, rows, piece), (n_tp, rows, piece), (n, cap, piece), (n, cap, piece),
        ((8, -(-tokens // 128) * 128), f32),
    ]
    semaphores = [
        (11,), (heads,), (1,), (n,), (n,), (n,), (n,), (n,), (n,), (n, g), (n,), (n, g), (n,), (n,), (n,),
        (n,), (n,), (g - 1,), (n,), (heads, n_tp), (n_tp, heads), (n_tp,), (n_tp,), (n_tp,), (n_tp,), (n_tp,), (n_tp,),
        (n,), (n,),
    ]
    return pl.pallas_call(
        functools.partial(mega_kernel, n, heads, n_tp, head_size),
        out_shape=(
            jax.ShapeDtypeStruct((rows, piece), bf16),
            jax.ShapeDtypeStruct((tokens, piece), bf16),
        ),
        in_specs=[pl.BlockSpec(memory_space=pltpu.SMEM)] + [vmem] * 4 + [any_spec, vmem] + [any_spec] * 11,
        out_specs=(vmem, vmem),
        scratch_shapes=[
            pltpu.VMEM(shape[0], shape[1]) if isinstance(shape[0], tuple) else pltpu.VMEM(shape, bf16)
            for shape in buffers
        ] + [dma(shape) for shape in semaphores],
        compiler_params=pltpu.CompilerParams(
            collective_id=0, has_side_effects=True, vmem_limit_bytes=60 * 2**20),
        cost_estimate=pl.CostEstimate(flops=30 * 10**9, bytes_accessed=24 * 2**20, transcendentals=6 * 10**6),
        name="exchange",
    )(
        head_lambda, head_gain.reshape(1, vw), routes.T, route_weight.T, ffn_gain.reshape(1, model),
        jnp.asarray(turns), jnp.asarray(bases), query_pairs, key_pairs, value_rows, moe_input, out_weight,
        gate_weight, up_weight, down_weight, shared_gate, shared_up, shared_down)


def local(
    query_pairs,
    key_pairs,
    value_rows,
    head_lambda,
    head_gain,
    out_weight,
    moe_input,
    ffn_gain,
    routes,
    route_weight,
    gate_weight,
    up_weight,
    down_weight,
    shared_gate,
    shared_up,
    shared_down,
):
    n = lax.axis_size("ep")
    heads = head_lambda.shape[0]
    rows = query_pairs.shape[0]
    fits = n == 2 * heads and heads % 2 == 0 and (rows * heads) % (n * 64) == 0
    if fits:
        return exchange_all(
            query_pairs, key_pairs, value_rows, head_lambda, head_gain, out_weight, moe_input, ffn_gain, routes,
            route_weight, gate_weight, up_weight, down_weight, shared_gate, shared_up, shared_down,
        )
    row_values = moe_input.astype(jnp.float32)
    inverse_norm = lax.rsqrt(jnp.mean(row_values * row_values, axis=-1, keepdims=True) + norm_eps)
    normed = (row_values * inverse_norm * ffn_gain).astype(jnp.bfloat16)
    attn_out = generic_attention(query_pairs, key_pairs, value_rows, head_lambda, head_gain, out_weight)
    token_rows = normed.shape[0]
    experts = lax.axis_size("ep")
    capacity = token_rows * TOP_K * 5 // (4 * experts)
    flat_routes = routes.reshape(-1)
    onehot = (flat_routes[:, None] == jnp.arange(experts, dtype=jnp.int32)).astype(jnp.int32)
    slot_rank = jnp.sum((jnp.cumsum(onehot, axis=0) - 1) * onehot, axis=-1)
    slot_index = flat_routes * capacity + slot_rank
    token_index = jnp.arange(token_rows * TOP_K, dtype=jnp.int32) // TOP_K
    slot_rows = (
        jnp.full((experts * capacity,), token_rows, jnp.int32).at[slot_index].set(token_index)
    )
    padded = jnp.concatenate([normed, jnp.zeros((1, normed.shape[1]), jnp.bfloat16)], axis=0)
    outgoing = padded[slot_rows]
    arrived = lax.all_to_all(outgoing, "ep", split_axis=0, concat_axis=0, tiled=True)
    gate_part = jnp.dot(arrived, gate_weight[0], preferred_element_type=jnp.float32)
    up_part = jnp.dot(arrived, up_weight[0], preferred_element_type=jnp.float32)
    hidden = (jax.nn.silu(gate_part) * up_part).astype(jnp.bfloat16)
    expert_terms = jnp.dot(hidden, down_weight[0], preferred_element_type=jnp.float32)
    shared_gated = jnp.dot(normed, shared_gate, preferred_element_type=jnp.float32)
    shared_lifted = jnp.dot(normed, shared_up, preferred_element_type=jnp.float32)
    shared_hidden = (jax.nn.silu(shared_gated) * shared_lifted).astype(jnp.bfloat16)
    shared_terms = jnp.dot(shared_hidden, shared_down, preferred_element_type=jnp.float32)
    expert_sum, shared_sum = (
        lax.psum_scatter(
            expert_terms.astype(jnp.bfloat16), "tp", scatter_dimension=1, tiled=True
        ).astype(jnp.float32),
        lax.psum_scatter(
            shared_terms.astype(jnp.bfloat16), "tp", scatter_dimension=1, tiled=True
        ).astype(jnp.float32),
    )
    returned = lax.all_to_all(
        expert_sum.astype(jnp.bfloat16), "ep", split_axis=0, concat_axis=0, tiled=True
    )
    picked = returned[slot_index.reshape(token_rows, TOP_K)]
    moe_out = (
        jnp.sum(route_weight[..., None] * picked.astype(jnp.float32), axis=1) + shared_sum
    ).astype(jnp.bfloat16)
    return (attn_out, moe_out)


def solution(mesh):
    return jax.shard_map(
        local,
        mesh=mesh,
        in_specs=(
            P("ep", "tp"),
            P("ep", "tp"),
            P("ep", "tp"),
            P("tp"),
            P(),
            P("tp", None),
            P("ep", None),
            P(),
            P("ep", None),
            P("ep", None),
            P("ep", None, "tp"),
            P("ep", None, "tp"),
            P("ep", "tp", None),
            P(None, "tp"),
            P(None, "tp"),
            P("tp", None),
        ),
        out_specs=(P("ep", "tp"), P("ep", "tp")),
        check_vma=False,
    )
```

time: 137 us -> 84.6 us (0.62); the launches traced: 135 us -> 83.8 us
  Pallas kernels: 125 us -> 79.8 us
  other arithmetic: 3.4 us -> 0 us
    pallas_call x3 -> x1, Pallas kernels: 125 us -> 79.8 us  [exchange_all(): pl.pallas_call(functools.partial(mega_kernel, n, heads, n_tp, head_size),...]
    unnamed x13 -> x2, local copies, waits for them, and re-layouts: 4.14 us -> 3.36 us
where the time goes in v1:
time: 84.6 us; the launch traced here: 83.8 us
  Pallas kernels  79.8 us (94%)
  local copies, waits for them, and re-layouts  3.36 us (4%)
    pallas_call x1, Pallas kernels, exchange_all(): pl.pallas_call(functools.partial(mega_kernel, n, heads, n_tp, head_size),...  79.8 us
    unnamed x2, local copies, waits for them, and re-layouts  3.36 us

profile of v1, /device:TPU:17, one launch (start us, length us, event | category | flops | bytes accessed | tf_op | source)
XLA Modules:
  0.0 83.8 jit_solution(1671580640791034571)
XLA Ops:
  0.6 79.8 %exchange.1 = (bf16[384,512]{1,0:T(8,128)(2,1)}, bf16[160,512]{1,0:T(8,128)(2,1)}) custom-call(f32[4]{0:T(128)} %lam_ref.1, f32[1,128]{1,0:T(1,128)} %bitcast.7, s32[2,160]{1,0:T(2,128)} %bitcast.5, f32[2,160]{1,0:T(2,128)} %bitcast.6, f32[1,2048]{1,0:T(1,128)} %bitcast.4, f32[2,384,128]{2,1,0:T(8,128)} %constant.4.clone.turn_ref, ...), custom_call_target="tpu_custom_call" | custom-call | flops 30000001024 | bytes 25165824 | tf_op jit(solution)/shard_map/exchange/pallas_call | solution.py:585
  80.4 1.8 %copy.22 = bf16[384,512]{1,0:T(8,128)(2,1)} copy(bf16[384,512]{1,0:T(8,128)(2,1)} %get-tuple-element.4) | data formatting | bytes 786432
  82.2 1.6 %copy.23 = bf16[160,512]{1,0:T(8,128)(2,1)} copy(bf16[160,512]{1,0:T(8,128)(2,1)} %get-tuple-element.5) | data formatting | bytes 327680

commit v2 on v1

--- a/solution.py
+++ b/solution.py
@@ -116,9 +116,9 @@
     attn_ref, moe_ref,
     q_in, k_in, v_in, turn, x_in, xn, place, rq, rk, q_buf, k_buf, v_buf, vt_buf, st_buf, acc, m_buf,
     hn_send, hn_buf, w_buf, out_buf, own_buf, arr, wg, wu, wd, sg, su, sd,
-    sh_send, sh_in, ex_send, ex_in, mix_send, mix_in, y_buf, ret, rw_pad,
-    load, load_v, barrier_free, q_ss, q_rs, k_ss, k_rs, v_ss, v_rs, fk_ss, fk_rs, fv_ss, fv_rs, h_ss, h_rs,
-    t_ss, t_rs, o_ss, o_rs, x_ss, x_rs, m_ss, m_rs, s_ss, s_rs, e_ss, e_rs, y_ss, y_rs,
+    sh_send, sh_in, ex_send, ex_first, ex_held, ex_second, mix_send, mix_first, mix_held, mix_second, y_buf, ret, rw_pad,
+    load, load_v, q_ss, q_rs, k_ss, k_rs, v_ss, v_rs, fk_ss, fk_rs, fv_ss, fv_rs, h_ss, h_rs,
+    t_ss, t_rs, o_ss, o_rs, x_ss, x_rs, d_ss, d_rs, m_ss, m_rs, m2_ss, m2_rs, s_ss, s_rs, e_ss, e_rs, e2_ss, e2_rs, y_ss, y_rs,
 ):
     me, my_tp = lax.axis_index("ep"), lax.axis_index("tp")
     g = n // heads
@@ -159,8 +159,6 @@
         copy.start()
     for copy in values:
         copy.start()
-    for copy in loads[4:]:
-        copy.start()
 
     def to_ep(source, target, send_sem, recv_sem, dest):
         return pltpu.make_async_remote_copy(
@@ -174,6 +172,34 @@
         to_ep(ref, ref, sem, sem, lax.rem(me + 1, n)).wait_recv()
 
     peers = [lax.rem(my_tp + step, n_tp) for step in (*range(1, n_tp), 0)]
+    across = (my_tp + 1 - 2 * (my_tp % 2), (my_tp + 2) % n_tp)
+    corner = (across[0] + 2) % n_tp
+
+    def reduction(send, first_in, held, second_in, ss, rs, ss2, rs2):
+        def first_copies(h):
+            return [
+                to_tp(send.at[dest, h], first_in.at[h, i], ss.at[h, i], rs.at[h, i], across[h])
+                for i, dest in enumerate((corner, across[h]))]
+
+        def second_copy(h):
+            return to_tp(held.at[h], second_in.at[h], ss2.at[h], rs2.at[h], across[1 - h])
+
+        def pass_on(h):
+            arrived(first_in.at[h, 0], rs.at[h, 0])
+            held[h] = (send[across[1 - h], h].astype(f32) + first_in[h, 0].astype(f32)).astype(bf16)
+            second_copy(h).start()
+
+        def total(h):
+            arrived(first_in.at[h, 1], rs.at[h, 1])
+            arrived(second_in.at[h], rs2.at[h])
+            return send[my_tp, h].astype(f32) + first_in[h, 1].astype(f32) + second_in[h].astype(f32)
+
+        def sent():
+            for h in range(2):
+                for copy in (*first_copies(h), second_copy(h)):
+                    copy.wait_send()
+
+        return first_copies, pass_on, total, sent
 
     def columns(t):
         return pl.ds(pl.multiple_of(t * piece, piece), piece)
@@ -202,6 +228,8 @@
         return jnp.dot(mark, xn[...], preferred_element_type=f32).astype(bf16)
 
     pl.semaphore_wait(barrier, n - 1 + n_tp - 1)
+    for copy in loads[4:]:
+        copy.start()
 
     def tok_copy(dest):
         return to_ep(out_buf.at[dest], arr.at[my_tp, me], t_ss.at[dest], t_rs.at[me], dest)
@@ -210,9 +238,20 @@
         dest = chip * g + lax.rem(core + step, g)
         return to_ep(own_buf.at[step - 1], arr.at[:, me], o_ss.at[step - 1], o_rs.at[me], dest)
 
-    for s in range(1, heads):
-        for c in range(g):
-            tok_copy(nearest(s) * g + c).start()
+    mate_chip = chip + 1 - 2 * (chip % 2)
+    inner = (chip + side) % 2
+
+    def send_tokens(first, last):
+        for s in range(first, last):
+            for c in range(g):
+                tok_copy(nearest(s) * g + c).start()
+
+    send_tokens(1, 2)
+
+    @pl.when(inner == 1)
+    def _():
+        send_tokens(2, heads)
+
     for step in range(g):
         full = own_rows(chip * g + lax.rem(core + step, g))
         for t in range(n_tp):
@@ -258,14 +297,36 @@
     def v_copy(dest):
         return to_ep(v_in.at[dest // g], v_buf.at[me], v_ss.at[dest], v_rs.at[me], dest)
 
-    for s in range(1, heads):
-        dest = nearest(s) * g + core
-        k_copy(dest).start()
+    def send_kv(p):
+        k_copy(p * g + core).start()
+        v_copy(p * g + core).start()
+
+    def send_q(p):
         for c in range(g):
-            q_copy(nearest(s) * g + c).start()
-        v_copy(dest).start()
+            q_copy(p * g + c).start()
+
     for step in range(1, g):
         q_copy(chip * g + lax.rem(core + step, g)).start()
+    send_kv(mate_chip)
+    send_q(mate_chip)
+
+    @pl.when(inner == 0)
+    def _():
+        send_tokens(2, heads)
+
+    @pl.when(side == 0)
+    def _():
+        for i in (0, 1):
+            send_kv(2 + (inner + i) % 2)
+            send_q(2 + (inner + i) % 2)
+
+    @pl.when(side == 1)
+    def _():
+        for s in range(2, heads):
+            send_q(nearest(s))
+        for i in (1, 0):
+            send_kv((inner + i) % 2)
+
     q_buf[me] = rq[chip, q_rows(me)]
     k_buf[me] = rk[chip]
     v_buf[me] = v_in[chip]
@@ -299,7 +360,11 @@
             to_ep(v_buf.at[source], v_buf.at[source], fv_ss.at[source, step], fv_rs.at[source], to),
         )
 
-    def receive(p):
+    def prepare_kv(e):
+        vt_buf[e, :vw] = v_buf[e].astype(f32).T.astype(bf16)
+        vt_buf[e, vw:] = jnp.ones((vt_rows - vw, rows), bf16)
+
+    def receive_kv(p):
         direct = p * g + core
 
         @pl.when(direct != me)
@@ -310,6 +375,16 @@
         for step in range(1, g):
             for copy in forward(direct, step):
                 copy.start()
+        prepare_kv(direct)
+
+    def complete_kv(p):
+        for step in range(1, g):
+            other = p * g + lax.rem(core + step, g)
+            arrived(k_buf.at[other], fk_rs.at[other])
+            arrived(v_buf.at[other], fv_rs.at[other])
+            prepare_kv(other)
+
+    def receive_q(p):
         for c in range(g):
             e = p * g + c
 
@@ -321,35 +396,25 @@
             zero = jnp.zeros_like(q)
             st_buf[p, 2 * c * sub : (2 * c + 1) * sub] = jnp.where(lane_row < width // 2, q, zero)
             st_buf[p, (2 * c + 1) * sub : (2 * c + 2) * sub] = jnp.where(lane_row < width // 2, zero, q)
-        for step in range(1, g):
-            other = p * g + lax.rem(core + step, g)
-            arrived(k_buf.at[other], fk_rs.at[other])
-            arrived(v_buf.at[other], fv_rs.at[other])
-        for c in range(g):
-            vt_buf[p, :vw, c * rows : (c + 1) * rows] = v_buf[p * g + c].astype(f32).T.astype(bf16)
-        vt_buf[p, vw:] = jnp.ones((vt_rows - vw, keys), bf16)
         m_buf[p] = jnp.full((1, keys), masked_low, f32)
         acc[p] = jnp.zeros((vt_rows, keys), f32)
 
-    def tile(p, j, diagonal):
-        for c in range(g):
-            first = c * rows if diagonal else 0
-            span = slice(first, keys)
-            size = keys - first
-            s = lax.dot_general(
-                k_buf[j * g + c], st_buf[p, span], (((1,), (1,)), ((), ())), preferred_element_type=f32)
-            if diagonal:
-                key = lax.broadcasted_iota(jnp.int32, (rows, size), 0) + c * rows
-                column = lax.broadcasted_iota(jnp.int32, (rows, size), 1) + first
-                block = column // rows
-                query = block * rows + column % sub + (core + block) % g * sub
-                s = jnp.where(key <= query, s, masked_low)
-            old = m_buf[p, :, span]
-            m = jnp.maximum(old, jnp.max(s, axis=0, keepdims=True))
-            weights = jnp.exp(s - m).astype(bf16)
-            m_buf[p, :, span] = m
-            acc[p, :, span] = acc[p, :, span] * jnp.exp(old - m) + jnp.dot(
-                vt_buf[j, :, c * rows : (c + 1) * rows], weights, preferred_element_type=f32)
+    def tile(p, e, first=0, diagonal=False):
+        span = slice(first, keys)
+        size = keys - first
+        s = lax.dot_general(k_buf[e], st_buf[p, span], (((1,), (1,)), ((), ())), preferred_element_type=f32)
+        if diagonal:
+            key = lax.broadcasted_iota(jnp.int32, (rows, size), 0) + first
+            column = lax.broadcasted_iota(jnp.int32, (rows, size), 1) + first
+            block = column // rows
+            query = block * rows + column % sub + (core + block) % g * sub
+            s = jnp.where(key <= query, s, masked_low)
+        old = m_buf[p, :, span]
+        m = jnp.maximum(old, jnp.max(s, axis=0, keepdims=True))
+        weights = jnp.exp(s - m).astype(bf16)
+        m_buf[p, :, span] = m
+        acc[p, :, span] = acc[p, :, span] * jnp.exp(old - m) + jnp.dot(
+            vt_buf[e], weights, preferred_element_type=f32)
 
     def hn_copy(dest):
         return to_ep(hn_send.at[dest], hn_buf.at[me], h_ss.at[dest], h_rs.at[me], dest)
@@ -366,63 +431,40 @@
             def _():
                 hn_copy(e).start()
 
-    def turn_of(p):
-        p = mirrored(p)
-        return jnp.where(p <= near, near - p, p)
-
-    def attend(s):
-        receive(nearest(s))
-
-        def queries(p, _):
-            def blocks(j, _):
-                @pl.when(jnp.maximum(turn_of(p), turn_of(j)) == s)
-                def _():
-                    tile(p, j, False)
-
-                return 0
-
-            @pl.when(turn_of(p) == s)
-            def _():
-                tile(p, p, True)
-
-            @pl.when(turn_of(p) <= s)
-            def _():
-                lax.fori_loop(0, p, blocks, 0)
-
-            last = 0
-            for j in range(heads):
-                last = jnp.maximum(last, jnp.where(j <= p, turn_of(j), 0))
-
-            @pl.when(last == s)
-            def _():
-                finish(p)
-
-            return 0
-
-        lax.fori_loop(0, heads, queries, 0)
-        return 0
-
-    def spread_copy(p, dest):
+    def spread_copy(p, i):
         part = arr.at[my_tp, pl.ds(p * g, g)]
-        return to_tp(part, part, x_ss.at[p, dest], x_rs.at[my_tp, p], dest)
+        return to_tp(part, part, x_ss.at[p, i], x_rs.at[my_tp, p], across[i])
+
+    def relay_copy(p, c):
+        part = arr.at[across[c], p * g + c]
+        return to_tp(part, part, d_ss.at[p, c], d_rs.at[p, c], across[1 - c])
 
     def spread(s):
         p = nearest(s)
         for c in range(g):
             arrived(arr.at[my_tp, p * g + c], t_rs.at[p * g + c])
-        for dest in peers[:-1]:
-            spread_copy(p, dest).start()
-
-    def ex_copy(dest):
-        return to_tp(ex_send.at[dest], ex_in.at[my_tp], e_ss.at[dest], e_rs.at[my_tp], dest)
+        for i in range(2):
+            spread_copy(p, i).start()
+
+    def relay(s):
+        p = nearest(s)
+        for c in range(2):
+            arrived(arr.at[across[c], pl.ds(p * g, g)], x_rs.at[across[c], p])
+            relay_copy(p, c).start()
+
+    ex_copies, ex_pass, ex_total, ex_sent = reduction(
+        ex_send, ex_first, ex_held, ex_second, e_ss, e_rs, e2_ss, e2_rs)
+    mix_copies, mix_pass, mix_total, mix_sent = reduction(
+        mix_send, mix_first, mix_held, mix_second, m_ss, m_rs, m2_ss, m2_rs)
+    half_rows = n // 2 * cap
 
     def routed():
         for step in range(1, g):
             other = chip * g + lax.rem(core + step, g)
             arrived(arr.at[:, other], o_rs.at[other])
         for s in range(1, heads):
-            for t in peers[:-1]:
-                arrived(arr.at[t, pl.ds(nearest(s) * g, g)], x_rs.at[t, nearest(s)])
+            for c in range(2):
+                arrived(arr.at[corner, nearest(s) * g + c], d_rs.at[nearest(s), c])
         for i in (7, 8, 9):
             loads[i].wait()
         gate = up = None
@@ -434,54 +476,142 @@
             gate = gate_part if gate is None else gate + gate_part
             up = up_part if up is None else up + up_part
         hidden = gated(gate, up)
-        for dest in peers:
-            ex_send[dest] = jnp.dot(hidden, wd[:, columns(dest)], preferred_element_type=f32).astype(bf16)
-            if dest is not peers[-1]:
-                ex_copy(dest).start()
+
+        def down(dest, h):
+            ex_send[dest, h] = jnp.dot(
+                hidden[h * half_rows : (h + 1) * half_rows], wd[:, columns(dest)],
+                preferred_element_type=f32).astype(bf16)
+
+        for i in range(2):
+            for h in range(2):
+                down((corner, across[h])[i], h)
+                ex_copies(h)[i].start()
+        for h in range(2):
+            down(across[1 - h], h)
+            down(my_tp, h)
+
+    low, pair = 1 - side, 2 * side
 
     def phase(s, _):
-        attend(s)
+        early = (4 - s) // 3
+        second = (s // 2) * (1 - s // 3)
+        third = (s // 3) * (1 - s // 4)
+        fourth = s // 4
+        newest = early * (chip + s * (mate_chip - chip)) + (1 - early) * (
+            low * (third * (2 + inner) + fourth * (3 - inner)) + side * (second * (1 - inner) + third * inner))
+        with_q = early + side * (second + third)
+        with_kv = with_q + low * (third + fourth)
+        split = third * (1 - inner) + fourth * inner
+
+        @pl.when(low * second == 1)
+        def _():
+            for p in (2, 3):
+                receive_q(p)
+
+        @pl.when(with_kv == 1)
+        def _():
+            receive_kv(newest)
+
+        @pl.when(with_q == 1)
+        def _():
+            receive_q(newest)
+
+        def diagonal(step, _):
+            c = (core + step) % g
+
+            @pl.when(step == 1)
+            def _():
+                complete_kv(newest)
+
+            for first in range(g):
+                @pl.when(c == first)
+                def _():
+                    tile(newest, newest * g + first, first * rows, True)
+
+            return 0
+
+        @pl.when(with_kv == 1)
+        def _():
+            lax.fori_loop(0, g, diagonal, 0)
+
+        @pl.when(low * (third * (1 - inner) + fourth) + side * (second * inner + third * (1 - inner)) == 1)
+        def _():
+            finish(newest)
+
+        def full(i, _):
+            p = early * (pair + 1) + second * (2 + low * (i // 2) + side * i) + low * split * 3 + side * third * (1 + i)
+            j = early * pair + second * (low * (i % 2) + side * newest) + low * split * 2 + side * third * newest * ((i + 1) // 2)
+            for c in range(g):
+                tile(p, j * g + c)
+
+            @pl.when(third * side + low * fourth * inner == 1)
+            def _():
+                finish(p)
+
+            return 0
+
+        lax.fori_loop(0, early * s + second * (4 * low + 2 * side) + low * split + side * third * 3, full, 0)
+
+        def done(p, _):
+            finish(p)
+            return 0
+
+        @pl.when(early * s * low == 1)
+        def _():
+            lax.fori_loop(pair, pair + 2, done, 0)
 
         @pl.when(s == 0)
         def _():
+            spread(1)
+
+        first = 1 - inner
+
+        @pl.when(s == 1 - first)
+        def _():
+            for step in range(2, heads):
+                spread(step)
             for step in range(1, heads):
-                spread(step)
+                relay(step)
 
         @pl.when(s == 1)
         def _():
             routed()
 
+        @pl.when(s == 2)
+        def _():
+            for h in range(2):
+                ex_pass(h)
+
         return 0
 
-    lax.fori_loop(0, heads, phase, 0)
+    lax.fori_loop(0, heads + 1, phase, 0)
 
     hn_buf[me] = hn_send[me]
     for step in range(1, n):
         source = lax.rem(me + step, n)
         arrived(hn_buf.at[source], h_rs.at[source])
     loads[10].wait()
-
-    def mix_copy(dest):
-        return to_tp(mix_send.at[dest], mix_in.at[my_tp], m_ss.at[dest], m_rs.at[my_tp], dest)
-
     normed = [
         jnp.concatenate([hn_buf[h * g + (part + n - me) % g] for h in range(heads)], axis=1) for part in range(g)]
-    for dest in peers:
-        for part in range(g):
-            mix_send[dest, part * sub : (part + 1) * sub] = jnp.dot(
-                normed[part], w_buf[:, columns(dest)], preferred_element_type=f32).astype(bf16)
-        if dest is not peers[-1]:
-            mix_copy(dest).start()
-
+
+    def project(dest, h):
+        mix_send[dest, h] = jnp.dot(normed[h], w_buf[:, columns(dest)], preferred_element_type=f32).astype(bf16)
+
+    for i in range(2):
+        for h in range(2):
+            project((corner, across[h])[i], h)
+            mix_copies(h)[i].start()
+    for h in range(2):
+        project(across[1 - h], h)
+        project(my_tp, h)
     def y_copy(dest):
         return to_ep(y_buf.at[dest], ret.at[me], y_ss.at[dest], y_rs.at[me], dest)
 
-    y = ex_send[my_tp].astype(f32)
-    for source in peers[:-1]:
-        arrived(ex_in.at[source], e_rs.at[source])
-        y = y + ex_in[source].astype(f32)
-    y_buf[...] = y.astype(bf16).reshape(n, cap, piece)
-    for s in range(1, heads):
+    for h in range(2):
+        y_buf[h * n // 2 : (h + 1) * n // 2] = ex_total(h).astype(bf16).reshape(n // 2, cap, piece)
+    for step in range(1, n):
+        hn_copy(lax.rem(me + step, n)).wait_send()
+    for s in range(heads - 1, 0, -1):
         for c in range(g):
             y_copy(nearest(s) * g + c).start()
     for step in range(1, g):
@@ -494,6 +624,8 @@
     rw_pad[...] = jnp.zeros_like(rw_pad)
     rw_pad[:top_k, :tokens] = rw_ref[...]
     scale = rw_pad[...].T
+    for h in range(2):
+        mix_pass(h)
     for step in range(1, n):
         source = lax.rem(me + step, n)
         arrived(ret.at[source], y_rs.at[source])
@@ -502,25 +634,20 @@
         out = out + scale[:tokens, k : k + 1] * lax.dot_general(
             place[k].reshape(n * cap, tokens), returned, (((0,), (0,)), ((), ())), preferred_element_type=f32)
     moe_ref[...] = out.astype(bf16)
-
-    total = mix_send[my_tp].astype(f32)
-    for source in peers[:-1]:
-        arrived(mix_in.at[source], m_rs.at[source])
-        total = total + mix_in[source].astype(f32)
-    attn_ref[...] = total.astype(bf16)
-
+    for h in range(2):
+        attn_ref[h * sub : (h + 1) * sub] = mix_total(h).astype(bf16)
     for s in range(1, heads):
         p = nearest(s)
         k_copy(p * g + core).wait_send()
         v_copy(p * g + core).wait_send()
         for c in range(g):
             tok_copy(p * g + c).wait_send()
-        for dest in peers[:-1]:
-            spread_copy(p, dest).wait_send()
+        for i in range(2):
+            spread_copy(p, i).wait_send()
+            relay_copy(p, i).wait_send()
     for step in range(1, n):
         dest = lax.rem(me + step, n)
         q_copy(dest).wait_send()
-        hn_copy(dest).wait_send()
         y_copy(dest).wait_send()
     for step in range(1, g):
         own_copy(step).wait_send()
@@ -530,8 +657,8 @@
                 copy.wait_send()
     for dest in peers[:-1]:
         sh_copy(dest).wait_send()
-        ex_copy(dest).wait_send()
-        mix_copy(dest).wait_send()
+    ex_sent()
+    mix_sent()
 
 
 def turn_tables(rows, n, head_size):
@@ -569,20 +696,21 @@
     buffers = [
         (rows, heads * width), (rows, heads * width), (heads, rows, vw), ((2, rows, width), f32),
         (tokens, model), (tokens, model), (TOP_K, n, cap, tokens), (heads, rows, width), (heads, rows, width),
-        (n, sub, width), (n, rows, width), (n, rows, vw), (heads, vw + 8, keys), (heads, 2 * rows, width),
+        (n, sub, width), (n, rows, width), (n, rows, vw), (n, vw + 8, rows), (heads, 2 * rows, width),
         ((heads, vw + 8, keys), f32), ((heads, 1, keys), f32), (n, sub, vw), (n, sub, vw), out_weight.shape,
         (n, cap, piece), (g - 1, n_tp, cap, piece), (n_tp, n, cap, piece),
         (model, hidden), (model, hidden), (hidden, model), (model, shared), (model, shared), (shared, model),
-        (n_tp, tokens, piece), (n_tp, tokens, piece), (n_tp, n * cap, piece), (n_tp, n * cap, piece),
-        (n_tp, rows, piece), (n_tp, rows, piece), (n, cap, piece), (n, cap, piece),
+        (n_tp, tokens, piece), (n_tp, tokens, piece),
+        (n_tp, 2, n // 2 * cap, piece), (2, 2, n // 2 * cap, piece), (2, n // 2 * cap, piece), (2, n // 2 * cap, piece),
+        (n_tp, 2, sub, piece), (2, 2, sub, piece), (2, sub, piece), (2, sub, piece), (n, cap, piece), (n, cap, piece),
         ((8, -(-tokens // 128) * 128), f32),
     ]
     semaphores = [
-        (11,), (heads,), (1,), (n,), (n,), (n,), (n,), (n,), (n,), (n, g), (n,), (n, g), (n,), (n,), (n,),
-        (n,), (n,), (g - 1,), (n,), (heads, n_tp), (n_tp, heads), (n_tp,), (n_tp,), (n_tp,), (n_tp,), (n_tp,), (n_tp,),
-        (n,), (n,),
+        (11,), (heads,), (n,), (n,), (n,), (n,), (n,), (n,), (n, g), (n,), (n, g), (n,), (n,), (n,),
+        (n,), (n,), (g - 1,), (n,), (heads, 2), (n_tp, heads), (heads, 2), (heads, 2),
+        (2, 2), (2, 2), (2,), (2,), (n_tp,), (n_tp,), (2, 2), (2, 2), (2,), (2,), (n,), (n,),
     ]
-    return pl.pallas_call(
+    results = pl.pallas_call(
         functools.partial(mega_kernel, n, heads, n_tp, head_size),
         out_shape=(
             jax.ShapeDtypeStruct((rows, piece), bf16),
@@ -602,6 +730,27 @@
         head_lambda, head_gain.reshape(1, vw), routes.T, route_weight.T, ffn_gain.reshape(1, model),
         jnp.asarray(turns), jnp.asarray(bases), query_pairs, key_pairs, value_rows, moe_input, out_weight,
         gate_weight, up_weight, down_weight, shared_gate, shared_up, shared_down)
+    return pl.pallas_call(
+        store_kernel,
+        out_shape=tuple(jax.ShapeDtypeStruct(r.shape, r.dtype) for r in results),
+        in_specs=[any_spec] * 2,
+        out_specs=(any_spec, any_spec),
+        scratch_shapes=[pltpu.VMEM(r.shape, r.dtype) for r in results] + [dma((2,)), dma((2,))],
+        name="store",
+    )(*results)
+
+
+def store_kernel(attn_ref, moe_ref, attn_out, moe_out, attn_buf, moe_buf, in_sems, out_sems):
+    refs = ((attn_ref, attn_buf, attn_out), (moe_ref, moe_buf, moe_out))
+    ins = [pltpu.make_async_copy(source, buf, in_sems.at[i]) for i, (source, buf, _) in enumerate(refs)]
+    outs = [pltpu.make_async_copy(buf, target, out_sems.at[i]) for i, (_, buf, target) in enumerate(refs)]
+    for copy in ins:
+        copy.start()
+    for i in (1, 0):
+        ins[i].wait()
+        outs[i].start()
+    for copy in outs:
+        copy.wait()
 
 
 def local(
@@ -625,7 +774,7 @@
     n = lax.axis_size("ep")
     heads = head_lambda.shape[0]
     rows = query_pairs.shape[0]
-    fits = n == 2 * heads and heads % 2 == 0 and (rows * heads) % (n * 64) == 0
+    fits = n == 2 * heads and heads == 4 and lax.axis_size("tp") == 4 and (rows * heads) % (n * 64) == 0
     if fits:
         return exchange_all(
             query_pairs, key_pairs, value_rows, head_lambda, head_gain, out_weight, moe_input, ffn_gain, routes,

time: 84.6 us -> 78.5 us (0.928)
  the two profiles are of different devices: /device:TPU:17 before, /device:TPU:25 now
where the time goes in v2:
time: 78.5 us; the launch traced here: 78.3 us
  Pallas kernels  77.7 us (99%)
    pallas_call x1, Pallas kernels, exchange_all(): pl.pallas_call(functools.partial(mega_kernel, n, heads, n_tp, head_size),...  75.8 us
    pallas_call x1, Pallas kernels, exchange_all(): pl.pallas_call(store_kernel, out_shape=tuple((jax.ShapeDtypeStruct(r.shap...  1.87 us

profile of v2, /device:TPU:25, one launch (start us, length us, event | category | flops | bytes accessed | tf_op | source)
XLA Modules:
  0.0 78.3 jit_solution(695170529416026901)
XLA Ops:
  0.6 75.8 %exchange.1 = (bf16[384,512]{1,0:T(8,128)(2,1)}, bf16[160,512]{1,0:T(8,128)(2,1)}) custom-call(f32[4]{0:T(128)} %lam_ref.1, f32[1,128]{1,0:T(1,128)} %bitcast.7, s32[2,160]{1,0:T(2,128)} %bitcast.5, f32[2,160]{1,0:T(2,128)} %bitcast.6, f32[1,2048]{1,0:T(1,128)} %bitcast.4, f32[2,384,128]{2,1,0:T(8,128)} %constant.4.clone.turn_ref, ...), custom_call_target="tpu_custom_call" | custom-call | flops 30000001024 | bytes 25165824 | tf_op jit(solution)/shard_map/exchange/pallas_call | solution.py:713
  76.5 1.9 %store.1 = (bf16[384,512]{1,0:T(8,128)(2,1)}, bf16[160,512]{1,0:T(8,128)(2,1)}) custom-call(bf16[384,512]{1,0:T(8,128)(2,1)} %get-tuple-element.4.attn_ref, bf16[160,512]{1,0:T(8,128)(2,1)} %get-tuple-element.5.moe_ref), custom_call_target="tpu_custom_call" | custom-call | tf_op jit(solution)/shard_map/store/pallas_call | solution.py:733

commit v3 on v2

--- a/solution.py
+++ b/solution.py
@@ -116,9 +116,9 @@
     attn_ref, moe_ref,
     q_in, k_in, v_in, turn, x_in, xn, place, rq, rk, q_buf, k_buf, v_buf, vt_buf, st_buf, acc, m_buf,
     hn_send, hn_buf, w_buf, out_buf, own_buf, arr, wg, wu, wd, sg, su, sd,
-    sh_send, sh_in, ex_send, ex_first, ex_held, ex_second, mix_send, mix_first, mix_held, mix_second, y_buf, ret, rw_pad,
+    sh_send, sh_first, sh_held, sh_second, ex_send, ex_first, ex_held, ex_second, mix_send, mix_first, mix_held, mix_second, y_buf, ret, rw_pad,
     load, load_v, q_ss, q_rs, k_ss, k_rs, v_ss, v_rs, fk_ss, fk_rs, fv_ss, fv_rs, h_ss, h_rs,
-    t_ss, t_rs, o_ss, o_rs, x_ss, x_rs, d_ss, d_rs, m_ss, m_rs, m2_ss, m2_rs, s_ss, s_rs, e_ss, e_rs, e2_ss, e2_rs, y_ss, y_rs,
+    t_ss, t_rs, o_ss, o_rs, x_ss, x_rs, d_ss, d_rs, m_ss, m_rs, m2_ss, m2_rs, s_ss, s_rs, s2_ss, s2_rs, e_ss, e_rs, e2_ss, e2_rs, y_ss, y_rs,
 ):
     me, my_tp = lax.axis_index("ep"), lax.axis_index("tp")
     g = n // heads
@@ -171,28 +171,31 @@
     def arrived(ref, sem):
         to_ep(ref, ref, sem, sem, lax.rem(me + 1, n)).wait_recv()
 
-    peers = [lax.rem(my_tp + step, n_tp) for step in (*range(1, n_tp), 0)]
     across = (my_tp + 1 - 2 * (my_tp % 2), (my_tp + 2) % n_tp)
     corner = (across[0] + 2) % n_tp
 
-    def reduction(send, first_in, held, second_in, ss, rs, ss2, rs2):
+    def reduction(send, first_in, held, second_in, ss, rs, ss2, rs2, pre=()):
+        at = lambda ref, *index: ref.at[(*pre, *index)]
+
         def first_copies(h):
             return [
-                to_tp(send.at[dest, h], first_in.at[h, i], ss.at[h, i], rs.at[h, i], across[h])
+                to_tp(at(send, dest, h), at(first_in, h, i), at(ss, h, i), at(rs, h, i), across[h])
                 for i, dest in enumerate((corner, across[h]))]
 
         def second_copy(h):
-            return to_tp(held.at[h], second_in.at[h], ss2.at[h], rs2.at[h], across[1 - h])
+            return to_tp(at(held, h), at(second_in, h), at(ss2, h), at(rs2, h), across[1 - h])
 
         def pass_on(h):
-            arrived(first_in.at[h, 0], rs.at[h, 0])
-            held[h] = (send[across[1 - h], h].astype(f32) + first_in[h, 0].astype(f32)).astype(bf16)
+            arrived(at(first_in, h, 0), at(rs, h, 0))
+            own = send[(*pre, across[1 - h], h)].astype(f32)
+            held[(*pre, h)] = (own + first_in[(*pre, h, 0)].astype(f32)).astype(bf16)
             second_copy(h).start()
 
         def total(h):
-            arrived(first_in.at[h, 1], rs.at[h, 1])
-            arrived(second_in.at[h], rs2.at[h])
-            return send[my_tp, h].astype(f32) + first_in[h, 1].astype(f32) + second_in[h].astype(f32)
+            arrived(at(first_in, h, 1), at(rs, h, 1))
+            arrived(at(second_in, h), at(rs2, h))
+            own = send[(*pre, my_tp, h)].astype(f32)
+            return own + first_in[(*pre, h, 1)].astype(f32) + second_in[(*pre, h)].astype(f32)
 
         def sent():
             for h in range(2):
@@ -339,13 +342,22 @@
     hidden = gated(
         jnp.dot(xn[...], sg[...], preferred_element_type=f32), jnp.dot(xn[...], su[...], preferred_element_type=f32))
 
-    def sh_copy(dest):
-        return to_tp(sh_send.at[dest], sh_in.at[my_tp], s_ss.at[dest], s_rs.at[my_tp], dest)
-
-    for dest in peers:
-        sh_send[dest] = jnp.dot(hidden, sd[:, columns(dest)], preferred_element_type=f32).astype(bf16)
-        if dest is not peers[-1]:
-            sh_copy(dest).start()
+    sh_copies, sh_pass, sh_total, sh_sent = reduction(
+        sh_send, sh_first, sh_held, sh_second, s_ss, s_rs, s2_ss, s2_rs)
+    half_tokens = tokens // 2
+
+    def shared_down(dest, h):
+        sh_send[dest, h] = jnp.dot(
+            hidden[h * half_tokens : (h + 1) * half_tokens], sd[:, columns(dest)],
+            preferred_element_type=f32).astype(bf16)
+
+    for i in range(2):
+        for h in range(2):
+            shared_down((corner, across[h])[i], h)
+            sh_copies(h)[i].start()
+    for h in range(2):
+        shared_down(across[1 - h], h)
+        shared_down(my_tp, h)
 
     lam = lam_ref[chip]
     gain = gain_ref[...]
@@ -452,40 +464,43 @@
             arrived(arr.at[across[c], pl.ds(p * g, g)], x_rs.at[across[c], p])
             relay_copy(p, c).start()
 
-    ex_copies, ex_pass, ex_total, ex_sent = reduction(
-        ex_send, ex_first, ex_held, ex_second, e_ss, e_rs, e2_ss, e2_rs)
+    expert_sums = [
+        reduction(ex_send, ex_first, ex_held, ex_second, e_ss, e_rs, e2_ss, e2_rs, (part,)) for part in range(2)]
     mix_copies, mix_pass, mix_total, mix_sent = reduction(
         mix_send, mix_first, mix_held, mix_second, m_ss, m_rs, m2_ss, m2_rs)
-    half_rows = n // 2 * cap
-
-    def routed():
-        for step in range(1, g):
-            other = chip * g + lax.rem(core + step, g)
-            arrived(arr.at[:, other], o_rs.at[other])
-        for s in range(1, heads):
+    def routed(part):
+        half = n // 2
+        start = half * (side if part == 0 else 1 - side)
+        if part == 0:
+            for step in range(1, g):
+                other = chip * g + lax.rem(core + step, g)
+                arrived(arr.at[:, other], o_rs.at[other])
+        for s in range(1, 2) if part == 0 else range(2, heads):
             for c in range(2):
                 arrived(arr.at[corner, nearest(s) * g + c], d_rs.at[nearest(s), c])
-        for i in (7, 8, 9):
-            loads[i].wait()
+        if part == 0:
+            for i in (7, 8, 9):
+                loads[i].wait()
         gate = up = None
         for t in range(n_tp):
-            block = arr[t].reshape(n * cap, piece)
+            block = arr[t, pl.ds(start, half)].reshape(half * cap, piece)
             span = slice(t * piece, (t + 1) * piece)
             gate_part = jnp.dot(block, wg[span, :], preferred_element_type=f32)
             up_part = jnp.dot(block, wu[span, :], preferred_element_type=f32)
             gate = gate_part if gate is None else gate + gate_part
             up = up_part if up is None else up + up_part
         hidden = gated(gate, up)
+        quarter = half // 2 * cap
 
         def down(dest, h):
-            ex_send[dest, h] = jnp.dot(
-                hidden[h * half_rows : (h + 1) * half_rows], wd[:, columns(dest)],
-                preferred_element_type=f32).astype(bf16)
-
+            ex_send[part, dest, h] = jnp.dot(
+                hidden[h * quarter : (h + 1) * quarter], wd[:, columns(dest)], preferred_element_type=f32).astype(bf16)
+
+        copies = expert_sums[part][0]
         for i in range(2):
             for h in range(2):
                 down((corner, across[h])[i], h)
-                ex_copies(h)[i].start()
+                copies(h)[i].start()
         for h in range(2):
             down(across[1 - h], h)
             down(my_tp, h)
@@ -498,10 +513,9 @@
         third = (s // 3) * (1 - s // 4)
         fourth = s // 4
         newest = early * (chip + s * (mate_chip - chip)) + (1 - early) * (
-            low * (third * (2 + inner) + fourth * (3 - inner)) + side * (second * (1 - inner) + third * inner))
+            low * (third * 3 + fourth * 2) + side * (second * (1 - inner) + third * inner))
         with_q = early + side * (second + third)
         with_kv = with_q + low * (third + fourth)
-        split = third * (1 - inner) + fourth * inner
 
         @pl.when(low * second == 1)
         def _():
@@ -534,57 +548,79 @@
         def _():
             lax.fori_loop(0, g, diagonal, 0)
 
-        @pl.when(low * (third * (1 - inner) + fourth) + side * (second * inner + third * (1 - inner)) == 1)
+        @pl.when(side * (second * inner + third * (1 - inner)) == 1)
         def _():
             finish(newest)
 
         def full(i, _):
-            p = early * (pair + 1) + second * (2 + low * (i // 2) + side * i) + low * split * 3 + side * third * (1 + i)
-            j = early * pair + second * (low * (i % 2) + side * newest) + low * split * 2 + side * third * newest * ((i + 1) // 2)
+            p = early * (pair + 1) + second * (2 + low * (i // 2) + side * i) + low * fourth * 3 + side * third * (1 + i)
+            j = early * pair + second * (low * (i % 2) + side * newest) + low * fourth * 2 + side * third * newest * ((i + 1) // 2)
             for c in range(g):
                 tile(p, j * g + c)
 
-            @pl.when(third * side + low * fourth * inner == 1)
+            @pl.when(third * side + low * fourth == 1)
             def _():
                 finish(p)
 
             return 0
 
-        lax.fori_loop(0, early * s + second * (4 * low + 2 * side) + low * split + side * third * 3, full, 0)
+        lax.fori_loop(0, early * s + second * (4 * low + 2 * side) + low * fourth + side * third * 3, full, 0)
 
         def done(p, _):
             finish(p)
             return 0
 
-        @pl.when(early * s * low == 1)
-        def _():
-            lax.fori_loop(pair, pair + 2, done, 0)
+        @pl.when((early * s + fourth) * low == 1)
+        def _():
+            lax.fori_loop(early * pair + fourth * 2, early * (pair + 2) + fourth * 3, done, 0)
 
         @pl.when(s == 0)
         def _():
             spread(1)
-
-        first = 1 - inner
-
-        @pl.when(s == 1 - first)
+            relay(1)
+
+        @pl.when(s == inner)
         def _():
             for step in range(2, heads):
                 spread(step)
-            for step in range(1, heads):
+
+        @pl.when(s == 1)
+        def _():
+            for step in range(2, heads):
                 relay(step)
-
-        @pl.when(s == 1)
-        def _():
-            routed()
+            routed(0)
+            routed(1)
+            for h in range(2):
+                expert_sums[0][1](h)
+                sh_pass(h)
 
         @pl.when(s == 2)
         def _():
             for h in range(2):
-                ex_pass(h)
+                expert_sums[1][1](h)
 
         return 0
 
     lax.fori_loop(0, heads + 1, phase, 0)
+
+    def y_copy(dest):
+        return to_ep(y_buf.at[dest], ret.at[me], y_ss.at[dest], y_rs.at[me], dest)
+
+    def send_back():
+        for part in (1, 0):
+            for h in range(2):
+                p = (side if part == 0 else 1 - side) * 2 + h
+                y_buf[pl.ds(p * g, g)] = expert_sums[part][2](h).astype(bf16).reshape(g, cap, piece)
+        for s in range(heads - 1, 0, -1):
+            for c in range(g):
+                y_copy(nearest(s) * g + c).start()
+        for step in range(1, g):
+            y_copy(chip * g + lax.rem(core + step, g)).start()
+        ret[me] = y_buf[me]
+
+    @pl.when(side == 1)
+    def _():
+        send_back()
 
     hn_buf[me] = hn_send[me]
     for step in range(1, n):
@@ -604,28 +640,17 @@
     for h in range(2):
         project(across[1 - h], h)
         project(my_tp, h)
-    def y_copy(dest):
-        return to_ep(y_buf.at[dest], ret.at[me], y_ss.at[dest], y_rs.at[me], dest)
-
     for h in range(2):
-        y_buf[h * n // 2 : (h + 1) * n // 2] = ex_total(h).astype(bf16).reshape(n // 2, cap, piece)
-    for step in range(1, n):
-        hn_copy(lax.rem(me + step, n)).wait_send()
-    for s in range(heads - 1, 0, -1):
-        for c in range(g):
-            y_copy(nearest(s) * g + c).start()
-    for step in range(1, g):
-        y_copy(chip * g + lax.rem(core + step, g)).start()
-    ret[me] = y_buf[me]
-    out = sh_send[my_tp].astype(f32)
-    for source in peers[:-1]:
-        arrived(sh_in.at[source], s_rs.at[source])
-        out = out + sh_in[source].astype(f32)
+        mix_pass(h)
+
+    @pl.when(side == 0)
+    def _():
+        send_back()
+
+    out = jnp.concatenate([sh_total(h) for h in range(2)], axis=0)
     rw_pad[...] = jnp.zeros_like(rw_pad)
     rw_pad[:top_k, :tokens] = rw_ref[...]
     scale = rw_pad[...].T
-    for h in range(2):
-        mix_pass(h)
     for step in range(1, n):
         source = lax.rem(me + step, n)
         arrived(ret.at[source], y_rs.at[source])
@@ -648,6 +673,7 @@
     for step in range(1, n):
         dest = lax.rem(me + step, n)
         q_copy(dest).wait_send()
+        hn_copy(dest).wait_send()
         y_copy(dest).wait_send()
     for step in range(1, g):
         own_copy(step).wait_send()
@@ -655,9 +681,9 @@
         for step in range(1, g):
             for copy in forward(p * g + core, step):
                 copy.wait_send()
-    for dest in peers[:-1]:
-        sh_copy(dest).wait_send()
-    ex_sent()
+    sh_sent()
+    for part in range(2):
+        expert_sums[part][3]()
     mix_sent()
 
 
@@ -700,15 +726,15 @@
         ((heads, vw + 8, keys), f32), ((heads, 1, keys), f32), (n, sub, vw), (n, sub, vw), out_weight.shape,
         (n, cap, piece), (g - 1, n_tp, cap, piece), (n_tp, n, cap, piece),
         (model, hidden), (model, hidden), (hidden, model), (model, shared), (model, shared), (shared, model),
-        (n_tp, tokens, piece), (n_tp, tokens, piece),
-        (n_tp, 2, n // 2 * cap, piece), (2, 2, n // 2 * cap, piece), (2, n // 2 * cap, piece), (2, n // 2 * cap, piece),
+        (n_tp, 2, tokens // 2, piece), (2, 2, tokens // 2, piece), (2, tokens // 2, piece), (2, tokens // 2, piece),
+        (2, n_tp, 2, g * cap, piece), (2, 2, 2, g * cap, piece), (2, 2, g * cap, piece), (2, 2, g * cap, piece),
         (n_tp, 2, sub, piece), (2, 2, sub, piece), (2, sub, piece), (2, sub, piece), (n, cap, piece), (n, cap, piece),
         ((8, -(-tokens // 128) * 128), f32),
     ]
     semaphores = [
         (11,), (heads,), (n,), (n,), (n,), (n,), (n,), (n,), (n, g), (n,), (n, g), (n,), (n,), (n,),
         (n,), (n,), (g - 1,), (n,), (heads, 2), (n_tp, heads), (heads, 2), (heads, 2),
-        (2, 2), (2, 2), (2,), (2,), (n_tp,), (n_tp,), (2, 2), (2, 2), (2,), (2,), (n,), (n,),
+        (2, 2), (2, 2), (2,), (2,), (2, 2), (2, 2), (2,), (2,), (2, 2, 2), (2, 2, 2), (2, 2), (2, 2), (n,), (n,),
     ]
     results = pl.pallas_call(
         functools.partial(mega_kernel, n, heads, n_tp, head_size),
@@ -774,7 +800,7 @@
     n = lax.axis_size("ep")
     heads = head_lambda.shape[0]
     rows = query_pairs.shape[0]
-    fits = n == 2 * heads and heads == 4 and lax.axis_size("tp") == 4 and (rows * heads) % (n * 64) == 0
+    fits = n == 2 * heads and heads == 4 and lax.axis_size("tp") == 4 and (rows * heads) % (n * 64) == 0 and routes.shape[0] % 32 == 0
     if fits:
         return exchange_all(
             query_pairs, key_pairs, value_rows, head_lambda, head_gain, out_weight, moe_input, ffn_gain, routes,

time: 78.5 us -> 77.9 us (level)
  the two profiles are of different devices: /device:TPU:25 before, /device:TPU:17 now
where the time goes in v3:
time: 77.9 us; the launch traced here: 77.7 us
  Pallas kernels  77 us (99%)
    pallas_call x1, Pallas kernels, exchange_all(): pl.pallas_call(functools.partial(mega_kernel, n, heads, n_tp, head_size),...  75.2 us
    pallas_call x1, Pallas kernels, exchange_all(): pl.pallas_call(store_kernel, out_shape=tuple((jax.ShapeDtypeStruct(r.shap...  1.87 us

profile of v3, /device:TPU:17, one launch (start us, length us, event | category | flops | bytes accessed | tf_op | source)
XLA Modules:
  0.0 77.7 jit_solution(5078149796758658325)
XLA Ops:
  0.6 75.2 %exchange.1 = (bf16[384,512]{1,0:T(8,128)(2,1)}, bf16[160,512]{1,0:T(8,128)(2,1)}) custom-call(f32[4]{0:T(128)} %lam_ref.1, f32[1,128]{1,0:T(1,128)} %bitcast.7, s32[2,160]{1,0:T(2,128)} %bitcast.5, f32[2,160]{1,0:T(2,128)} %bitcast.6, f32[1,2048]{1,0:T(1,128)} %bitcast.4, f32[2,384,128]{2,1,0:T(8,128)} %constant.4.clone.turn_ref, ...), custom_call_target="tpu_custom_call" | custom-call | flops 30000001024 | bytes 25165824 | tf_op jit(solution)/shard_map/exchange/pallas_call | solution.py:739
  75.8 1.9 %store.1 = (bf16[384,512]{1,0:T(8,128)(2,1)}, bf16[160,512]{1,0:T(8,128)(2,1)}) custom-call(bf16[384,512]{1,0:T(8,128)(2,1)} %get-tuple-element.4.attn_ref, bf16[160,512]{1,0:T(8,128)(2,1)} %get-tuple-element.5.moe_ref), custom_call_target="tpu_custom_call" | custom-call | tf_op jit(solution)/shard_map/store/pallas_call | solution.py:759

commit v4 on v3

--- a/solution.py
+++ b/solution.py
@@ -111,9 +111,10 @@
 
 
 def mega_kernel(
-    n, heads, n_tp, head_size, lam_ref, gain_ref, routes_ref, rw_ref, ffn_ref, turn_ref, base_ref,
+    n, heads, n_tp, head_size, lam_hbm, gain_hbm, routes_hbm, rw_hbm, ffn_hbm, turn_ref, base_hbm,
     q_ref, k_ref, v_ref, x_ref, w_ref, wg_ref, wu_ref, wd_ref, sg_ref, su_ref, sd_ref,
-    attn_ref, moe_ref,
+    attn_hbm, moe_hbm,
+    lam_ref, gain_ref, routes_ref, rw_ref, ffn_ref, base_ref, attn_ref, moe_ref, small, out_sem,
     q_in, k_in, v_in, turn, x_in, xn, place, rq, rk, q_buf, k_buf, v_buf, vt_buf, st_buf, acc, m_buf,
     hn_send, hn_buf, w_buf, out_buf, own_buf, arr, wg, wu, wd, sg, su, sd,
     sh_send, sh_first, sh_held, sh_second, ex_send, ex_first, ex_held, ex_second, mix_send, mix_first, mix_held, mix_second, y_buf, ret, rw_pad,
@@ -155,9 +156,12 @@
     values = [
         pltpu.make_async_copy(v_ref.at[:, h * vw : (h + 1) * vw], v_in.at[h], load_v.at[h]) for h in range(heads)
     ]
-    for copy in loads[:4]:
-        copy.start()
-    for copy in values:
+    smalls = [
+        pltpu.make_async_copy(source, target, small.at[i])
+        for i, (source, target) in enumerate((
+            (routes_hbm, routes_ref), (ffn_hbm, ffn_ref), (base_hbm, base_ref),
+            (lam_hbm, lam_ref), (gain_hbm, gain_ref), (rw_hbm, rw_ref)))]
+    for copy in (smalls[0], loads[0], *smalls[1:3], *loads[1:4], *values, *smalls[3:]):
         copy.start()
 
     def to_ep(source, target, send_sem, recv_sem, dest):
@@ -207,6 +211,7 @@
     def columns(t):
         return pl.ds(pl.multiple_of(t * piece, piece), piece)
 
+    smalls[0].wait()
     expert = lax.broadcasted_iota(jnp.int32, (n, tokens), 0)
     chosen = [(routes_ref[k : k + 1, :] == expert).astype(f32) for k in range(top_k)]
     earlier = lax.broadcasted_iota(jnp.int32, (tokens, tokens), 0) <= lax.broadcasted_iota(jnp.int32, (tokens, tokens), 1)
@@ -218,6 +223,7 @@
     for k in range(top_k):
         place[k] = marks[k].astype(bf16).reshape(n, cap, tokens)
     loads[0].wait()
+    smalls[1].wait()
     x = x_in[...].astype(f32)
     inverse = lax.rsqrt(jnp.mean(x * x, axis=-1, keepdims=True) + norm_eps)
     xn[...] = (x * inverse * ffn_ref[...]).astype(bf16)
@@ -266,6 +272,7 @@
         if step:
             own_copy(step).start()
 
+    smalls[2].wait()
     base_cos, base_sin = base_ref[0, pl.ds(me, 1)], base_ref[1, pl.ds(me, 1)]
     lane = lax.broadcasted_iota(jnp.int32, (1, width), 1)
     front = lane % head_size < half
@@ -359,6 +366,8 @@
         shared_down(across[1 - h], h)
         shared_down(my_tp, h)
 
+    for copy in smalls[3:]:
+        copy.wait()
     lam = lam_ref[chip]
     gain = gain_ref[...]
     vt_rows = vt_buf.shape[1]
@@ -508,23 +517,29 @@
     low, pair = 1 - side, 2 * side
 
     def phase(s, _):
-        early = (4 - s) // 3
+        early = (5 - s) // 4
         second = (s // 2) * (1 - s // 3)
         third = (s // 3) * (1 - s // 4)
-        fourth = s // 4
+        fourth = (s // 4) * (1 - s // 5)
+        fifth = s // 5
         newest = early * (chip + s * (mate_chip - chip)) + (1 - early) * (
-            low * (third * 3 + fourth * 2) + side * (second * (1 - inner) + third * inner))
+            low * (third * 3 + (fourth + fifth) * 2) + side * (second * (1 - inner) + third * inner))
         with_q = early + side * (second + third)
-        with_kv = with_q + low * (third + fourth)
+        with_kv = with_q + low * (third + fifth)
 
         @pl.when(low * second == 1)
         def _():
             for p in (2, 3):
                 receive_q(p)
 
-        @pl.when(with_kv == 1)
+        @pl.when(with_kv - low * fifth == 1)
         def _():
             receive_kv(newest)
+
+        @pl.when(low * fourth == 1)
+        def _():
+            receive_kv(2)
+            complete_kv(2)
 
         @pl.when(with_q == 1)
         def _():
@@ -533,7 +548,7 @@
         def diagonal(step, _):
             c = (core + step) % g
 
-            @pl.when(step == 1)
+            @pl.when(step * (1 - fifth) == 1)
             def _():
                 complete_kv(newest)
 
@@ -570,9 +585,9 @@
             finish(p)
             return 0
 
-        @pl.when((early * s + fourth) * low == 1)
-        def _():
-            lax.fori_loop(early * pair + fourth * 2, early * (pair + 2) + fourth * 3, done, 0)
+        @pl.when((early * s + fifth) * low == 1)
+        def _():
+            lax.fori_loop(early * pair + fifth * 2, early * (pair + 2) + fifth * 3, done, 0)
 
         @pl.when(s == 0)
         def _():
@@ -601,7 +616,7 @@
 
         return 0
 
-    lax.fori_loop(0, heads + 1, phase, 0)
+    lax.fori_loop(0, heads + 2, phase, 0)
 
     def y_copy(dest):
         return to_ep(y_buf.at[dest], ret.at[me], y_ss.at[dest], y_rs.at[me], dest)
@@ -659,8 +674,11 @@
         out = out + scale[:tokens, k : k + 1] * lax.dot_general(
             place[k].reshape(n * cap, tokens), returned, (((0,), (0,)), ((), ())), preferred_element_type=f32)
     moe_ref[...] = out.astype(bf16)
+    moe_store = pltpu.make_async_copy(moe_ref, moe_hbm, out_sem.at[2])
+    moe_store.start()
     for h in range(2):
-        attn_ref[h * sub : (h + 1) * sub] = mix_total(h).astype(bf16)
+        attn_ref[h] = mix_total(h).astype(bf16)
+        pltpu.make_async_copy(attn_ref.at[h], attn_hbm.at[h * sub : (h + 1) * sub], out_sem.at[h]).start()
     for s in range(1, heads):
         p = nearest(s)
         k_copy(p * g + core).wait_send()
@@ -685,6 +703,9 @@
     for part in range(2):
         expert_sums[part][3]()
     mix_sent()
+    moe_store.wait()
+    for h in range(2):
+        pltpu.make_async_copy(attn_ref.at[h], attn_hbm.at[h * sub : (h + 1) * sub], out_sem.at[h]).wait()
 
 
 def turn_tables(rows, n, head_size):
@@ -717,7 +738,6 @@
     hidden, shared = gate_weight.shape[2], shared_gate.shape[1]
     turns, bases = turn_tables(rows, n, head_size)
     any_spec = pl.BlockSpec(memory_space=pl.ANY)
-    vmem = pl.BlockSpec(memory_space=pltpu.VMEM)
     dma = pltpu.SemaphoreType.DMA
     buffers = [
         (rows, heads * width), (rows, heads * width), (heads, rows, vw), ((2, rows, width), f32),
@@ -742,9 +762,13 @@
             jax.ShapeDtypeStruct((rows, piece), bf16),
             jax.ShapeDtypeStruct((tokens, piece), bf16),
         ),
-        in_specs=[pl.BlockSpec(memory_space=pltpu.SMEM)] + [vmem] * 4 + [any_spec, vmem] + [any_spec] * 11,
-        out_specs=(vmem, vmem),
+        in_specs=[any_spec] * 18,
+        out_specs=(any_spec, any_spec),
         scratch_shapes=[
+            pltpu.SMEM((heads,), f32), pltpu.VMEM((1, vw), f32), pltpu.VMEM((TOP_K, tokens), jnp.int32),
+            pltpu.VMEM((TOP_K, tokens), f32), pltpu.VMEM((1, model), f32), pltpu.VMEM(bases.shape, f32),
+            pltpu.VMEM((2, sub, piece), bf16), pltpu.VMEM((tokens, piece), bf16), dma((6,)), dma((3,)),
+        ] + [
             pltpu.VMEM(shape[0], shape[1]) if isinstance(shape[0], tuple) else pltpu.VMEM(shape, bf16)
             for shape in buffers
         ] + [dma(shape) for shape in semaphores],

time: 77.9 us -> 76 us (0.976)
  Pallas kernels: 77 us -> 75.2 us
    pallas_call x1, Pallas kernels: 75.2 us -> 73.4 us  [exchange_all(): pl.pallas_call(functools.partial(mega_kernel, n, heads, n_tp, head_size),...]
where the time goes in v4:
time: 76 us; the launch traced here: 75.9 us
  Pallas kernels  75.2 us (99%)
    pallas_call x1, Pallas kernels, exchange_all(): pl.pallas_call(functools.partial(mega_kernel, n, heads, n_tp, head_size),...  73.4 us
    pallas_call x1, Pallas kernels, exchange_all(): pl.pallas_call(store_kernel, out_shape=tuple((jax.ShapeDtypeStruct(r.shap...  1.87 us

profile of v4, /device:TPU:17, one launch (start us, length us, event | category | flops | bytes accessed | tf_op | source)
XLA Modules:
  0.0 75.9 jit_solution(12072774570482891022)
XLA Ops:
  0.6 73.4 %exchange.1 = (bf16[384,512]{1,0:T(8,128)(2,1)}, bf16[160,512]{1,0:T(8,128)(2,1)}) custom-call(f32[4]{0:T(128)} %lam_hbm.1, f32[1,128]{1,0:T(1,128)} %bitcast.7, s32[2,160]{1,0:T(2,128)} %bitcast.5, f32[2,160]{1,0:T(2,128)} %bitcast.6, f32[1,2048]{1,0:T(1,128)} %bitcast.4, f32[2,384,128]{2,1,0:T(8,128)} %constant.4.clone.turn_ref, ...), custom_call_target="tpu_custom_call" | custom-call | flops 30000001024 | bytes 25165824 | tf_op jit(solution)/shard_map/exchange/pallas_call | solution.py:759
  74.0 1.9 %store.1 = (bf16[384,512]{1,0:T(8,128)(2,1)}, bf16[160,512]{1,0:T(8,128)(2,1)}) custom-call(bf16[384,512]{1,0:T(8,128)(2,1)} %get-tuple-element.4.attn_ref, bf16[160,512]{1,0:T(8,128)(2,1)} %get-tuple-element.5.moe_ref), custom_call_target="tpu_custom_call" | custom-call | tf_op jit(solution)/shard_map/store/pallas_call | solution.py:783

commit v5 on v4

--- a/solution.py
+++ b/solution.py
@@ -599,17 +599,20 @@
             for step in range(2, heads):
                 spread(step)
 
-        @pl.when(s == 1)
+        @pl.when(s == 1 + low * inner)
         def _():
             for step in range(2, heads):
                 relay(step)
             routed(0)
+
+        @pl.when(s == 1 + low * inner)
+        def _():
             routed(1)
             for h in range(2):
                 expert_sums[0][1](h)
                 sh_pass(h)
 
-        @pl.when(s == 2)
+        @pl.when(s == 2 + 2 * low * inner)
         def _():
             for h in range(2):
                 expert_sums[1][1](h)

time: 76 us -> 73.8 us (0.971)
  Pallas kernels: 75.2 us -> 72.9 us
    pallas_call x1, Pallas kernels: 73.4 us -> 71.1 us  [exchange_all(): pl.pallas_call(functools.partial(mega_kernel, n, heads, n_tp, head_size),...]
where the time goes in v5:
time: 73.8 us; the launch traced here: 73.6 us
  Pallas kernels  72.9 us (99%)
    pallas_call x1, Pallas kernels, exchange_all(): pl.pallas_call(functools.partial(mega_kernel, n, heads, n_tp, head_size),...  71.1 us
    pallas_call x1, Pallas kernels, exchange_all(): pl.pallas_call(store_kernel, out_shape=tuple((jax.ShapeDtypeStruct(r.shap...  1.87 us

profile of v5, /device:TPU:17, one launch (start us, length us, event | category | flops | bytes accessed | tf_op | source)
XLA Modules:
  0.0 73.6 jit_solution(8880801180935357013)
XLA Ops:
  0.6 71.1 %exchange.1 = (bf16[384,512]{1,0:T(8,128)(2,1)}, bf16[160,512]{1,0:T(8,128)(2,1)}) custom-call(f32[4]{0:T(128)} %lam_hbm.1, f32[1,128]{1,0:T(1,128)} %bitcast.7, s32[2,160]{1,0:T(2,128)} %bitcast.5, f32[2,160]{1,0:T(2,128)} %bitcast.6, f32[1,2048]{1,0:T(1,128)} %bitcast.4, f32[2,384,128]{2,1,0:T(8,128)} %constant.4.clone.turn_ref, ...), custom_call_target="tpu_custom_call" | custom-call | flops 30000001024 | bytes 25165824 | tf_op jit(solution)/shard_map/exchange/pallas_call | solution.py:762
  71.7 1.9 %store.1 = (bf16[384,512]{1,0:T(8,128)(2,1)}, bf16[160,512]{1,0:T(8,128)(2,1)}) custom-call(bf16[384,512]{1,0:T(8,128)(2,1)} %get-tuple-element.4.attn_ref, bf16[160,512]{1,0:T(8,128)(2,1)} %get-tuple-element.5.moe_ref), custom_call_target="tpu_custom_call" | custom-call | tf_op jit(solution)/shard_map/store/pallas_call | solution.py:786

commit v6 on v5

--- a/solution.py
+++ b/solution.py
@@ -658,10 +658,14 @@
     for h in range(2):
         project(across[1 - h], h)
         project(my_tp, h)
+    @pl.when(low * inner == 1)
+    def _():
+        send_back()
+
     for h in range(2):
         mix_pass(h)
 
-    @pl.when(side == 0)
+    @pl.when(low * (1 - inner) == 1)
     def _():
         send_back()
 

time: 73.8 us -> 73.8 us (level)
  no operation moved by 1% of the time
where the time goes in v6:
time: 73.8 us; the launch traced here: 73.6 us
  Pallas kernels  72.9 us (99%)
    pallas_call x1, Pallas kernels, exchange_all(): pl.pallas_call(functools.partial(mega_kernel, n, heads, n_tp, head_size),...  71.1 us
    pallas_call x1, Pallas kernels, exchange_all(): pl.pallas_call(store_kernel, out_shape=tuple((jax.ShapeDtypeStruct(r.shap...  1.87 us

profile of v6, /device:TPU:17, one launch (start us, length us, event | category | flops | bytes accessed | tf_op | source)
XLA Modules:
  0.0 73.6 jit_solution(7605382550501433804)
XLA Ops:
  0.6 71.1 %exchange.1 = (bf16[384,512]{1,0:T(8,128)(2,1)}, bf16[160,512]{1,0:T(8,128)(2,1)}) custom-call(f32[4]{0:T(128)} %lam_hbm.1, f32[1,128]{1,0:T(1,128)} %bitcast.7, s32[2,160]{1,0:T(2,128)} %bitcast.5, f32[2,160]{1,0:T(2,128)} %bitcast.6, f32[1,2048]{1,0:T(1,128)} %bitcast.4, f32[2,384,128]{2,1,0:T(8,128)} %constant.4.clone.turn_ref, ...), custom_call_target="tpu_custom_call" | custom-call | flops 30000001024 | bytes 25165824 | tf_op jit(solution)/shard_map/exchange/pallas_call | solution.py:766
  71.7 1.9 %store.1 = (bf16[384,512]{1,0:T(8,128)(2,1)}, bf16[160,512]{1,0:T(8,128)(2,1)}) custom-call(bf16[384,512]{1,0:T(8,128)(2,1)} %get-tuple-element.4.attn_ref, bf16[160,512]{1,0:T(8,128)(2,1)} %get-tuple-element.5.moe_ref), custom_call_target="tpu_custom_call" | custom-call | tf_op jit(solution)/shard_map/store/pallas_call | solution.py:790
